TPU v7x, 512 devices: a whole 4x4x16 slice. The times are simulated.
512 devices in a mesh: sp: 64 (over z, y), tp: 8 (over x, core).
Axes of the slice: x: 4, y: 4, z: 16, core: 2. Of those that a mesh axis runs over, the one named last changes fastest.
Arguments:
- tokens: bfloat16 [32768, 3072], P('sp'), may hold values from -72 to 72
- w_query: bfloat16 [3072, 1024], P('sp', 'tp'), may hold values from -0.109375 to 0.109375
- w_key: bfloat16 [3072, 1024], P('sp', 'tp'), may hold values from -0.109375 to 0.109375
- w_value: bfloat16 [3072, 1024], P('sp', 'tp'), may hold values from -0.4375 to 0.4375
- w_out: bfloat16 [1024, 3072], P('tp', 'sp'), may hold values from -0.1875 to 0.1875
Outputs:
- mixed: bfloat16 [32768, 3072], P(('sp', 'tp'))
- row_lse: float32 [16, 32768], P('tp', 'sp')
All inputs are finite; a program needn't handle non-finite values.
Results may differ from a plain program's by a relative error of at most 0.014.
Values may be sent and summed in bfloat16 or wider, within the bound.
A program may use at most 64 MiB of HBM per device.

v0:
```python
from functools import partial

import jax
import jax.numpy as jnp
from jax import lax
from jax.sharding import Mesh
from jax.sharding import PartitionSpec as P

HEAD_SIZE = 64
KEYS_BEHIND = 128
SP = ("sp_0", "sp_1")
SP_TP = ("sp_0", "sp_1", "tp")


dilation_rates = (1, 4, 16)
neg_big = -1e30


def sent_together(arrays, axis, dim, along):
    widths = [a.shape[along] for a in arrays]
    both = jnp.concatenate(arrays, axis=along)
    result = lax.all_gather(both, axis, axis=dim, tiled=True)
    return tuple(jnp.split(result, [sum(widths[:k]) for k in range(1, len(widths))], axis=along))


def passed_along(block, axis, distance):
    devices = range(lax.axis_size(axis))
    route = [(i - distance, i) for i in devices if i - distance in devices]
    return lax.ppermute(block, axis, route)


def whole_of(shard, axes, dim):
    for axis in reversed(axes):
        shard = lax.all_gather(shard, axis, axis=dim, tiled=True)
    return shard


def in_blocks(shard, dim, count):
    before, after = (shard.shape[:dim], shard.shape[dim + 1 :])
    return jnp.moveaxis(shard.reshape(*before, count, -1, *after), dim, 0)


def summed_on_arrival(shard, axis, dim):
    count = lax.axis_size(axis)
    pieces = lax.all_to_all(in_blocks(shard, dim, count), axis, 0, 0, tiled=True)
    return jnp.sum(pieces.astype(jnp.float32), axis=0)


def band(query_class_rows, key_class_rows, value_class_rows, key_first_index):
    sequence_length = query_class_rows.shape[0]
    if sequence_length <= KEYS_BEHIND:
        blocks = 1
        step = sequence_length
        q_blk = query_class_rows[None]
        k_blk = key_class_rows[None]
        v_blk = value_class_rows[None]
    else:
        blocks = sequence_length // KEYS_BEHIND
        step = KEYS_BEHIND
        q_blk = query_class_rows.reshape(blocks, KEYS_BEHIND, HEAD_SIZE)
        k_rows = key_class_rows.reshape(blocks + 1, KEYS_BEHIND, HEAD_SIZE)
        v_rows = value_class_rows.reshape(blocks + 1, KEYS_BEHIND, HEAD_SIZE)
        k_blk = jnp.concatenate([k_rows[:-1], k_rows[1:]], axis=1)
        v_blk = jnp.concatenate([v_rows[:-1], v_rows[1:]], axis=1)
    score = jnp.einsum(
        "nqd,nkd->nqk", q_blk, k_blk, preferred_element_type=jnp.float32
    ) * HEAD_SIZE ** (-0.5)
    row_at = jnp.arange(step, dtype=jnp.int32)[:, None]
    col_at = jnp.arange(k_blk.shape[1], dtype=jnp.int32)[None, :]
    dist = KEYS_BEHIND + row_at - col_at
    key_pos = (
        key_first_index + jnp.arange(blocks, dtype=jnp.int32)[:, None, None] * step + col_at[None]
    )
    mask = (dist >= 0) & (dist <= KEYS_BEHIND) & (key_pos >= 0)
    score = jnp.where(mask, score, neg_big)
    top = jnp.max(score, axis=-1, keepdims=True)
    weight = jnp.exp(score - top)
    denom = jnp.sum(weight, axis=-1)
    weight_bf = weight.astype(jnp.bfloat16)
    out = (
        jnp.einsum("nqk,nkd->nqd", weight_bf, v_blk, preferred_element_type=jnp.float32)
        / denom[..., None]
    )
    lse = top[..., 0] + jnp.log(denom)
    return (out.reshape(sequence_length, HEAD_SIZE), lse.reshape(sequence_length))


def shards(tokens, w_query, w_key, w_value, w_out):
    row_indices = tokens.shape[0]
    width = w_query.shape[1]
    head_outputs = width // HEAD_SIZE
    pieces = sent_together((w_query, w_key, w_value), SP, 0, 1)
    q_sum, k_sum, v_sum = tuple(
        (jnp.dot(tokens, piece, preferred_element_type=jnp.float32) for piece in pieces)
    )
    query_input = q_sum.astype(jnp.bfloat16)
    keys = k_sum.astype(jnp.bfloat16)
    values = v_sum.astype(jnp.bfloat16)
    widest = KEYS_BEHIND * 16
    reach = (widest + row_indices - 1) // row_indices
    prior_keys, prior_values = passed_along((keys, values), SP, 1)
    for level in range((reach - 1).bit_length()):
        far_keys, far_values = passed_along((prior_keys, prior_values), SP, 1 << level)
        prior_keys = jnp.concatenate([far_keys, prior_keys], 0)
        prior_values = jnp.concatenate([far_values, prior_values], 0)
    base_offset = lax.axis_index(SP) * row_indices
    outs = []
    lses = []
    for dilation_rate in dilation_rates:
        window_keys = KEYS_BEHIND * dilation_rate
        sequence_length = row_indices // dilation_rate
        held = prior_keys.shape[0]
        key_all_rows = jnp.concatenate([prior_keys[held - window_keys :], keys], 0)
        value_all_rows = jnp.concatenate([prior_values[held - window_keys :], values], 0)
        query_class_rows = query_input.reshape(
            sequence_length, dilation_rate, head_outputs, HEAD_SIZE
        ).transpose(1, 2, 0, 3)
        key_class_rows = key_all_rows.reshape(
            KEYS_BEHIND + sequence_length, dilation_rate, head_outputs, HEAD_SIZE
        ).transpose(1, 2, 0, 3)
        value_class_rows = value_all_rows.reshape(
            KEYS_BEHIND + sequence_length, dilation_rate, head_outputs, HEAD_SIZE
        ).transpose(1, 2, 0, 3)
        key_first_index = base_offset // dilation_rate - KEYS_BEHIND
        banded = partial(band, key_first_index=key_first_index)
        out, lse = jax.vmap(jax.vmap(banded))(query_class_rows, key_class_rows, value_class_rows)
        outs.append(out.transpose(2, 0, 1, 3).reshape(row_indices, head_outputs, HEAD_SIZE))
        lses.append(lse.transpose(1, 2, 0).reshape(head_outputs, row_indices))
    lse_all = jnp.stack(lses, 0)
    peak = jnp.max(lse_all, axis=0)
    expo = jnp.exp(lse_all - peak)
    total = jnp.sum(expo, axis=0)
    mix = (expo / total).transpose(0, 2, 1)
    attended = jnp.sum(mix[..., None] * jnp.stack(outs, 0), axis=0)
    attended = attended.reshape(row_indices, width).astype(jnp.bfloat16)
    row_lse = peak + jnp.log(total)
    full_out = whole_of(w_out, SP, 1)
    mixed = summed_on_arrival(
        jnp.dot(attended, full_out, preferred_element_type=jnp.float32).astype(jnp.bfloat16),
        "tp",
        0,
    ).astype(jnp.bfloat16)
    return (mixed, row_lse)


def solution(mesh):
    torus = Mesh(mesh.devices.reshape(16, 4, mesh.shape["tp"]), ("sp_0", "sp_1", "tp"))
    in_specs = (P(SP, None), P(SP, "tp"), P(SP, "tp"), P(SP, "tp"), P("tp", SP))
    out_specs = (P(SP_TP, None), P("tp", SP))
    return jax.shard_map(
        shards, mesh=torus, in_specs=in_specs, out_specs=out_specs, check_vma=False
    )
```

profile of v0, /device:TPU:1, one launch (start us, length us, event | category | flops | bytes accessed | tf_op | source)
XLA Modules:
  0.0 322.1 jit_solution(11991866663673161450)
XLA Ops:
  7.2 1.5 pad_maximum_fusion.8
  8.8 10.6 %all_gather.10 = bf16[128,192]{0,1:T(8,128)(2,1)S(1)} all-gather(bf16[128,48]{0,1:T(8,128)(2,1)} %param.9), channel_id=1, replica_groups=mesh['sp_0'=16,'sp_1'=4,'tp'=8] {'sp_1'}, dimensions={1}, use_global_device_ids=true | all-gather | bytes 61440 | tf_op jit(solution)/shard_map/all_gather | solution.py:34
  20.2 0.7 fusion.36
  20.9 0.7 broadcast_and_fusion
  21.6 36.9 %all_gather.11 = bf16[128,3072]{0,1:T(8,128)(2,1)} all-gather(bf16[128,192]{0,1:T(8,128)(2,1)S(1)} %all_gather.10), channel_id=1, replica_groups=mesh['sp_0'=16,'sp_1'=4,'tp'=8] {'sp_0'}, dimensions={1}, use_global_device_ids=true | all-gather | bytes 835584 | tf_op jit(solution)/shard_map/all_gather | solution.py:34
  58.5 90.2 %all-gather.2.cloned.1.call-done = bf16[3072,384]{1,0:T(8,128)(2,1)} async-done(((bf16[48,384]{1,0:T(8,128)(2,1)}), bf16[3072,384]{1,0:T(8,128)(2,1)}) %all-gather.2.cloned.1.call-update) | async-done | bytes 2359312 | tf_op jit(solution)/shard_map/all_gather | solution.py:22
  148.7 2.5 fusion.5
  151.2 2.7 collective-permute-start
  153.9 1.2 fusion.6
  155.1 1.9 convolution_convert_fusion.3
  157.0 1.0 copy.45
  158.0 0.9 reshape.353
  158.8 0.9 reshape.351
  159.7 1.6 reshape.347
  161.3 2.8 collective-permute-start.3
  164.1 0.8 slice.24
  164.9 0.7 pad_maximum_fusion.6
  165.6 1.8 reshape.349
  167.4 1.1 fusion.48
  169.2 0.7 copy.69
  169.9 0.8 slice.27
  170.6 0.7 pad_maximum_fusion.7
  171.3 1.8 reshape.356
  173.1 1.1 fusion.47
  174.3 1.5 fusion.51
  176.6 0.9 copy.59
  177.5 1.8 reshape.358
  179.3 3.1 collective-permute-start.1
  183.0 4.2 %collective-permute-start.4 = (bf16[512,128]{0,1:T(8,128)(2,1)}, bf16[512,128]{0,1:T(8,128)(2,1)}, u32[]{:S(2)}, u32[]{:S(2)}) collective-permute-start(bf16[512,128]{0,1:T(8,128)(2,1)} %collective-permute-done.3), channel_id=1, source_target_pairs={{0,8},{8,16},{16,24},{24,32},{32,40},{40,48},{48,56},{56,64},{64,7... | collective-permute-start | bytes 393224 | tf_op jit(solution)/shard_map/ppermute | solution.py:29
  187.2 1.9 pad_maximum_fusion.2
  189.0 1.8 copy.46
  190.8 2.0 reshape.352
  192.8 1.9 copy.47
  194.7 1.4 fusion.50
  196.2 1.0 copy-done.2
  197.7 0.7 stack_reshape.21
  198.4 0.7 stack_reshape.19
  199.1 1.9 pad_maximum_fusion.4
  201.0 1.8 copy.60
  202.8 2.1 reshape.359
  204.8 1.9 copy.61
  206.7 3.7 %collective-permute-start.5 = (bf16[1024,128]{0,1:T(8,128)(2,1)}, bf16[1024,128]{0,1:T(8,128)(2,1)}, u32[]{:S(2)}, u32[]{:S(2)}) collective-permute-start(bf16[1024,128]{0,1:T(8,128)(2,1)} %get-tuple-element.9), channel_id=1, source_target_pairs={{0,16},{8,24},{16,32},{24,40},{32,48},{40,56},{48,64},{56,72},{64,... | collective-permute-start | bytes 786440 | tf_op jit(solution)/shard_map/ppermute | solution.py:29
  210.5 3.8 %collective-permute-start.2 = (bf16[1024,128]{0,1:T(8,128)(2,1)}, bf16[1024,128]{0,1:T(8,128)(2,1)}, u32[]{:S(2)}, u32[]{:S(2)}) collective-permute-start(bf16[1024,128]{0,1:T(8,128)(2,1)} %get-tuple-element.11), channel_id=1, source_target_pairs={{0,16},{8,24},{16,32},{24,40},{32,48},{40,56},{48,64},{56,72},{64,... | collective-permute-start | bytes 786440 | tf_op jit(solution)/shard_map/ppermute | solution.py:29
  214.3 2.3 fusion.4
  216.6 1.9 copy.62
  218.6 1.9 copy.66
  220.5 1.9 pad_maximum_fusion
  222.4 2.2 copy.51
  224.6 3.7 %reshape.354 = bf16[160,16,2,64]{3,2,1,0:T(2,128)(2,1)} reshape(bf16[2560,128]{1,0:T(8,128)(2,1)} %copy.51) | data formatting | bytes 1310720 | tf_op jit(solution)/shard_map/reshape | solution.py:118
  228.3 3.8 %copy.52 = bf16[160,16,2,64]{0,3,2,1:T(8,128)(2,1)} copy(bf16[160,16,2,64]{3,2,1,0:T(2,128)(2,1)} %reshape.354) | data formatting | bytes 1310720 | tf_op jit(solution)/shard_map/reshape | solution.py:118
  232.1 1.6 fusion.49
  233.7 1.0 copy-done.1
  235.4 2.0 pad_maximum_fusion.1
  237.4 2.2 copy.63
  239.5 3.6 %reshape.360 = bf16[160,16,2,64]{3,2,1,0:T(2,128)(2,1)} reshape(bf16[2560,128]{1,0:T(8,128)(2,1)} %copy.63) | data formatting | bytes 1310720 | tf_op jit(solution)/shard_map/reshape | solution.py:121
  243.2 3.8 %copy.64 = bf16[160,16,2,64]{0,3,2,1:T(8,128)(2,1)} copy(bf16[160,16,2,64]{3,2,1,0:T(2,128)(2,1)} %reshape.360) | data formatting | bytes 1310720 | tf_op jit(solution)/shard_map/reshape | solution.py:121
  247.0 2.0 fusion.3
  249.0 1.1 copy.65
  250.1 1.9 copy.67
  252.2 1.1 fusion.18
  253.3 3.8 %convolution_convert_fusion = bf16[512,3072]{1,0:T(8,128)(2,1)} fusion(bf16[512,128]{0,1:T(8,128)(2,1)S(1)} %bitcast.101, bf16[128,3072]{0,1:T(8,128)(2,1)} %all_gather.11), kind=kOutput, calls=%fused_computation | convolution fusion | flops 404226048 | bytes 4063232 | tf_op jit(solution)/shard_map/dot_general | solution.py:139
  257.1 17.3 %all-to-all-start = ((bf16[8,64,3072]{2,1,0:T(8,128)(2,1)}), bf16[8,64,3072]{2,1,0:T(8,128)(2,1)}, u32[]{:S(2)}, u32[]{:S(2)}) async-start(bf16[8,64,3072]{2,1,0:T(8,128)(2,1)} %bitcast.91), calls=%async_computation | async-start | bytes 6291456 | tf_op jit(solution)/shard_map/all_to_all | solution.py:45
  275.0 37.0 %all-to-all-done = bf16[8,64,3072]{2,1,0:T(8,128)(2,1)} async-done(((bf16[8,64,3072]{2,1,0:T(8,128)(2,1)}), bf16[8,64,3072]{2,1,0:T(8,128)(2,1)}, u32[]{:S(2)}, u32[]{:S(2)}) %all-to-all-start) | async-done | bytes 3145760 | tf_op jit(solution)/shard_map/all_to_all | solution.py:45
  311.9 3.3 %reduce_sum.62 = bf16[64,3072]{1,0:T(8,128)(2,1)} reduce(bf16[8,64,3072]{2,1,0:T(8,128)(2,1)} %all-to-all-done, bf16[]{:T(256)} %constant.76.clone.1), dimensions={0}, to_apply=%region_8.9 | reduce | flops 1376256 | bytes 3538946 | tf_op jit(solution)/shard_map/reduce_sum | solution.py:46
  (60 shorter events, 4.9 us)
Async XLA Ops:
  7.2 141.5 %copy-start = (bf16[512,3072]{1,0:T(8,128)(2,1)S(1)}, bf16[512,3072]{1,0:T(8,128)(2,1)}, u32[]{:S(2)}) copy-start(bf16[512,3072]{1,0:T(8,128)(2,1)} %param.5) | copy-start | bytes 9437188
  7.2 141.5 %all-gather.2.cloned.1.call-start = ((), (), s32[]{:S(2)}) async-start(), calls=%async_computation.1 | async-start | bytes 2396160 | tf_op jit(solution)/shard_map/all_gather | solution.py:22
  148.7 5.2 %copy-start.3 = (bf16[3072,384]{1,0:T(8,128)(2,1)S(1)}, bf16[3072,384]{1,0:T(8,128)(2,1)}, u32[]{:S(2)}) copy-start(bf16[3072,384]{1,0:T(8,128)(2,1)} %all-gather.2.cloned.1.call-done) | copy-start | bytes 7077892
  151.2 13.0 %collective-permute-start = (bf16[512,128]{0,1:T(8,128)(2,1)S(1)}, bf16[512,128]{0,1:T(8,128)(2,1)}, u32[]{:S(2)}, u32[]{:S(2)}) collective-permute-start(bf16[512,128]{0,1:T(8,128)(2,1)S(1)} %fusion.5), channel_id=1, source_target_pairs={{0,8},{8,16},{16,24},{24,32},{32,40},{40,48},{48,56},{56,64},{64,7... | collective-permute-start | bytes 393224 | tf_op jit(solution)/shard_map/ppermute | solution.py:29
  159.7 14.6 %copy-start.8 = (pred[4,128,256]{2,1,0:T(8,128)(4,1)S(1)}, pred[4,128,256]{2,1,0:T(8,128)(4,1)}, u32[]{:S(2)}) copy-start(pred[4,128,256]{2,1,0:T(8,128)(4,1)} %broadcast_and_fusion) | copy-start | bytes 393220
  161.3 8.6 %collective-permute-start.3 = (bf16[512,128]{0,1:T(8,128)(2,1)S(1)}, bf16[512,128]{0,1:T(8,128)(2,1)}, u32[]{:S(2)}, u32[]{:S(2)}) collective-permute-start(bf16[512,128]{0,1:T(8,128)(2,1)S(1)} %fusion.6), channel_id=1, source_target_pairs={{0,8},{8,16},{16,24},{24,32},{32,40},{40,48},{48,56},{56,64},{64,7... | collective-permute-start | bytes 393224 | tf_op jit(solution)/shard_map/ppermute | solution.py:29
  179.3 7.9 %collective-permute-start.1 = (bf16[512,128]{0,1:T(8,128)(2,1)}, bf16[512,128]{0,1:T(8,128)(2,1)S(1)}, u32[]{:S(2)}, u32[]{:S(2)}) collective-permute-start(bf16[512,128]{0,1:T(8,128)(2,1)} %collective-permute-done), channel_id=1, source_target_pairs={{0,8},{8,16},{16,24},{24,32},{32,40},{40,48},{48,56},{56,64},{64,7... | collective-permute-start | bytes 393224 | tf_op jit(solution)/shard_map/ppermute | solution.py:29
  182.4 12.3 %copy-start.9 = (f32[1,8,128]{2,1,0:T(8,128)}, f32[1,8,128]{2,1,0:T(8,128)S(1)}, u32[]{:S(2)}) copy-start(f32[1,8,128]{2,1,0:T(8,128)S(1)} %log_add_fusion.1) | copy-start | bytes 12292
  183.0 16.1 %collective-permute-start.4 = (bf16[512,128]{0,1:T(8,128)(2,1)}, bf16[512,128]{0,1:T(8,128)(2,1)}, u32[]{:S(2)}, u32[]{:S(2)}) collective-permute-start(bf16[512,128]{0,1:T(8,128)(2,1)} %collective-permute-done.3), channel_id=1, source_target_pairs={{0,8},{8,16},{16,24},{24,32},{32,40},{40,48},{48,56},{56,64},{64,7... | collective-permute-start | bytes 393224 | tf_op jit(solution)/shard_map/ppermute | solution.py:29
  187.2 10.3 %copy-start.6 = (bf16[512,128]{0,1:T(8,128)(2,1)}, bf16[512,128]{0,1:T(8,128)(2,1)S(1)}, u32[]{:S(2)}) copy-start(bf16[512,128]{0,1:T(8,128)(2,1)S(1)} %collective-permute-done.1) | copy-start | bytes 393220
  196.1 1.0 copy-start.2
  202.8 17.7 %copy-start.7 = (bf16[512,128]{0,1:T(8,128)(2,1)S(1)}, bf16[512,128]{0,1:T(8,128)(2,1)}, u32[]{:S(2)}) copy-start(bf16[512,128]{0,1:T(8,128)(2,1)} %copy-done.6) | copy-start | bytes 393220
  206.7 28.7 %collective-permute-start.5 = (bf16[1024,128]{0,1:T(8,128)(2,1)}, bf16[1024,128]{0,1:T(8,128)(2,1)}, u32[]{:S(2)}, u32[]{:S(2)}) collective-permute-start(bf16[1024,128]{0,1:T(8,128)(2,1)} %get-tuple-element.9), channel_id=1, source_target_pairs={{0,16},{8,24},{16,32},{24,40},{32,48},{40,56},{48,64},{56,72},{64,... | collective-permute-start | bytes 786440 | tf_op jit(solution)/shard_map/ppermute | solution.py:29
  210.5 10.0 %collective-permute-start.2 = (bf16[1024,128]{0,1:T(8,128)(2,1)}, bf16[1024,128]{0,1:T(8,128)(2,1)}, u32[]{:S(2)}, u32[]{:S(2)}) collective-permute-start(bf16[1024,128]{0,1:T(8,128)(2,1)} %get-tuple-element.11), channel_id=1, source_target_pairs={{0,16},{8,24},{16,32},{24,40},{32,48},{40,56},{48,64},{56,72},{64,... | collective-permute-start | bytes 786440 | tf_op jit(solution)/shard_map/ppermute | solution.py:29
  224.6 7.5 %copy-start.5 = (bf16[32,16,2,64]{3,2,1,0:T(2,128)(2,1)S(1)}, bf16[32,16,2,64]{3,2,1,0:T(2,128)(2,1)}, u32[]{:S(2)}) copy-start(bf16[32,16,2,64]{3,2,1,0:T(2,128)(2,1)} %reshape.353) | copy-start | bytes 393220
  233.7 1.0 copy-start.1
  247.0 5.1 %copy-start.10 = (f32[1,8,128]{2,1,0:T(8,128)S(1)}, f32[1,8,128]{2,1,0:T(8,128)}, u32[]{:S(2)}) copy-start(f32[1,8,128]{2,1,0:T(8,128)} %copy-done.9) | copy-start | bytes 12292
  247.0 5.1 %copy-start.11 = (f32[2,512]{1,0:T(2,128)S(1)}, f32[2,512]{1,0:T(2,128)}, u32[]{:S(2)}) copy-start(f32[2,512]{1,0:T(2,128)} %stack_reshape.21) | copy-start | bytes 12292
  247.0 5.1 %copy-start.12 = (f32[1,2,512]{2,1,0:T(2,128)S(1)}, f32[1,2,512]{2,1,0:T(2,128)}, u32[]{:S(2)}) copy-start(f32[1,2,512]{2,1,0:T(2,128)} %stack_reshape.19) | copy-start | bytes 12292
  247.0 5.1 %copy-start.13 = (f32[1,2,512]{2,1,0:T(2,128)S(1)}, f32[1,2,512]{2,1,0:T(2,128)}, u32[]{:S(2)}) copy-start(f32[1,2,512]{2,1,0:T(2,128)} %add.141) | copy-start | bytes 12292
  247.0 5.2 %copy-start.4 = (f32[1,512,2,64]{1,3,2,0:T(8,128)S(1)}, f32[1,512,2,64]{1,3,2,0:T(8,128)}, u32[]{:S(2)}) copy-start(f32[1,512,2,64]{1,3,2,0:T(8,128)} %copy.66) | copy-start | bytes 786436
  257.1 54.9 %all-to-all-start = ((bf16[8,64,3072]{2,1,0:T(8,128)(2,1)}), bf16[8,64,3072]{2,1,0:T(8,128)(2,1)}, u32[]{:S(2)}, u32[]{:S(2)}) async-start(bf16[8,64,3072]{2,1,0:T(8,128)(2,1)} %bitcast.91), calls=%async_computation | async-start | bytes 6291456 | tf_op jit(solution)/shard_map/all_to_all | solution.py:45
Sparse Core Ops, SparseCore 0:
  11.5 137.1 all-gather.1
where the time goes:
time: 324 us; the launch traced here: 322 us
  waiting for transfers between devices  127 us (39%)
  local copies, waits for them, and re-layouts  57.8 us (18%)
  blocking collectives  47.5 us (15%)
  starting transfers between devices  37.8 us (12%)
  other arithmetic  18.9 us (6%)
  matrix products  18.6 us (6%)
  between operations  14.3 us (4%)
    all_gather x1, waiting for transfers between devices, sent_together(): result = lax.all_gather(both, axis, axis=dim, tiled=True)  90.2 us
    all_gather x2, blocking collectives, whole_of(): shard = lax.all_gather(shard, axis, axis=dim, tiled=True)  47.5 us
    all_to_all x1, waiting for transfers between devices, summed_on_arrival(): lax.all_to_all(in_blocks(shard, dim, count), axis, 0, 0, tiled=True)  37 us
    ppermute x6, starting transfers between devices, passed_along(): return lax.ppermute(block, axis, route)  20.4 us
    all_to_all x1, starting transfers between devices, summed_on_arrival(): lax.all_to_all(in_blocks(shard, dim, count), axis, 0, 0, tiled=True)  17.3 us
    reshape x4, local copies, waits for them, and re-layouts, shards(): value_all_rows.reshape(KEYS_BEHIND + sequence_length, dilation_rate, head...  11.4 us
    reshape x4, local copies, waits for them, and re-layouts, shards(): key_all_rows.reshape(KEYS_BEHIND + sequence_length, dilation_rate, head_o...  11.3 us
  transfers between devices with their start and end apart: 8, of which 2 were waited for; matrix products, arithmetic and copies ran while one was open for 15% of the time, Pallas kernels for 0%

commit v1 on v0

v1 whole, which is shorter than its diff:
```python
import jax
import jax.numpy as jnp
from jax import lax
from jax.experimental import pallas as pl
from jax.experimental.pallas import tpu as pltpu
from jax.sharding import Mesh
from jax.sharding import PartitionSpec as P

HEAD = 64
WINDOW = 128
NZ = 16
NY = 4
NX = 4
MESH = pl.DeviceIdType.MESH
SP = ("z", "y")
TP = ("x", "c")
NEG = -1e30
LN2 = 0.6931471805599453
F32 = jnp.float32
BF16 = jnp.bfloat16


def nt_dot(a, b):
    return lax.dot_general(a, b, (((1,), (1,)), ((), ())), preferred_element_type=F32)


def remote(src, dst, send, recv, device):
    return pltpu.make_async_remote_copy(
        src_ref=src, dst_ref=dst, send_sem=send, recv_sem=recv, device_id=device, device_id_type=MESH
    )


def layer_kernel(
    tokens, wq, wk, wv, wo, mixed, lse_out,
    tok, wkv, wqo, wox, halo, qf, kvf, oa, ma, la, att, lse_rows, att_b, att_x, part, part_b, part_x,
    bias_a, bias_b,
    tok_sem, kvy_s, kvy_r, zs, zr, ys, yr, xs, xr, hs, hr, as_, ar, cs, cr,
):
    z, y, x, c = (lax.axis_index(n) for n in ("z", "y", "x", "c"))
    sp = z * NY + y
    shard, lanes = wk.shape
    rows = tokens.shape[0]
    copy_tokens = pltpu.make_async_copy(tokens, tok, tok_sem)
    copy_tokens.start()

    def at_z(d):
        return lax.rem(z + d + NZ, NZ)

    def at_y(d):
        return lax.rem(y + d + NY, NY)

    def at_x(d):
        return lax.rem(x + d + NX, NX)

    wkv[sp, :, 0:lanes] = wk[...]
    wkv[sp, :, lanes:] = wv[...]
    wqo[sp, :, 0:lanes] = wq[...]
    wqo[sp, :, lanes:] = wo[...]

    barrier = pltpu.get_barrier_semaphore()
    peers = [{"z": at_z(1)}, {"z": at_z(-1)}]
    peers += [{"y": at_y(d)} for d in range(1, NY)]
    peers += [{"x": at_x(d)} for d in range(1, NX)]
    peers += [{"c": 1 - c}]
    for peer in peers:
        pl.semaphore_signal(barrier, inc=1, device_id=peer, device_id_type=MESH)
    pl.semaphore_wait(barrier, len(peers))

    sends = []

    def start(cp):
        cp.start()
        sends.append(cp)

    z_up, z_dn = {"z": at_z(1)}, {"z": at_z(-1)}
    y_up, y_dn = {"y": at_y(1)}, {"y": at_y(-1)}

    def half(ref, flow, h):
        part_ = pl.ds(h * lanes, lanes)
        return ref.at[:, :, part_] if flow == 0 else ref.at[:, part_]

    def z_block(flow, src):
        return wkv.at[pl.ds(src * NY, NY)] if flow == 0 else wqo.at[src * NY + y]

    last = NZ // 2

    def z_copy(flow, way, s, src_z):
        ref = z_block(flow, src_z)
        if s == last:
            ref = half(ref, flow, way)
        return remote(ref, ref, zs.at[flow, way, s - 1], zr.at[flow, way, s - 1], z_up if way == 0 else z_dn)

    def z_send(flow, way, s):
        start(z_copy(flow, way, s, at_z(-(s - 1) if way == 0 else s - 1)))

    def z_wait(flow, way, s):
        z_copy(flow, way, s, at_z(-s if way == 0 else s)).wait_recv()

    def y_copy(kind, slot, col):
        src_z = at_z(-slot)
        ref = wqo.at[src_z * NY + at_y(col)]
        if kind >= 2:
            ref = half(ref, 1, kind - 2)
        return remote(ref, ref, ys.at[kind, slot], yr.at[kind, slot], y_up if kind % 2 == 0 else y_dn)

    def y_send(slot):
        start(y_copy(0, slot, 0))
        start(y_copy(1, slot, 0))

    def y_relay(slot):
        y_copy(0, slot, -1).wait_recv()
        start(y_copy(2, slot, -1))
        y_copy(1, slot, 1).wait_recv()
        start(y_copy(3, slot, 1))

    def y_done(slot):
        y_copy(2, slot, 2).wait_recv()
        y_copy(3, slot, 2).wait_recv()

    def kv_row(d, col):
        ref = wkv.at[sp + 0 * col] if col is None else wkv.at[z * NY + at_y(col)]
        return remote(ref, ref, kvy_s.at[d - 1], kvy_r.at[d - 1], {"y": at_y(d)})

    for d in (1, 3, 2):
        start(kv_row(d, 0))
    z_send(1, 0, 1)
    z_send(1, 1, 1)
    y_send(0)
    for d in (1, 3, 2):
        kv_row(d, -d).wait_recv()
    z_send(0, 0, 1)
    z_send(0, 1, 1)
    waiting = [0]
    for s in range(1, last + 1):
        for way in (0, 1):
            z_wait(1, way, s)
            if s < last:
                z_send(1, way, s + 1)
        arrived = [s, NZ - s] if s < last else [s]
        for slot in arrived:
            y_send(slot)
        for way in (0, 1):
            z_wait(0, way, s)
            if s < last:
                z_send(0, way, s + 1)
        for slot in waiting:
            y_relay(slot)
        waiting = arrived
    for slot in waiting:
        y_relay(slot)
    for slot in range(NZ):
        y_done(slot)

    chunks = wox.shape[1] // 16
    def x_copy(kind, k, rel):
        span = pl.ds(k * 16, 16)
        src = wqo.at[span, :, pl.ds(lanes, lanes)] if rel is None else wox.at[rel, span]
        place = {0: NX - 2, 1: 0, 2: 1, 3: 1}[kind]
        dst = wox.at[place, span]
        to = {"x": at_x(1)} if kind % 2 == 0 else {"x": at_x(-1)}
        j = kind if kind < 2 else 2
        return remote(src, dst, xs.at[j, k], xr.at[j, k], to)

    for k in range(chunks):
        start(x_copy(0, k, None))
        start(x_copy(1, k, None))

    def x_relay(k):
        up = k < chunks // 2
        x_copy(0, k, None).wait_recv()
        if up:
            start(x_copy(2, k, 2))
        x_copy(1, k, None).wait_recv()
        if not up:
            start(x_copy(3, k, 0))

    copy_tokens.wait()
    kv = jnp.dot(tok[...], wkv[...].reshape(NZ * NY * shard, 2 * lanes), preferred_element_type=F32)
    for j in range(2):
        side = slice(j * lanes, (j + 1) * lanes)
        kvf[j, WINDOW:, :] = kv[:, side]
        for e in range(4):
            for b in range(4):
                picked = kvf[j, pl.ds(WINDOW + 4 * b + e, 32, stride=16), :]
                halo[e, 0, 32 * b:32 * b + 32, side] = picked.astype(BF16)

    def prev_copy(e):
        return remote(halo.at[e, 0], halo.at[e, 4], hs.at[0, e], hr.at[0, e], z_up)

    def row_copy(e, k, src):
        return remote(halo.at[e, src], halo.at[e, k], hs.at[k, e], hr.at[k, e], {"y": at_y(k)})

    for e in range(4):
        prev_copy(e).start()
    for k in (1, 3, 2):
        @pl.when(y + k < NY)
        def _():
            for e in range(4):
                row_copy(e, k, 0).start()

    q = jnp.dot(tok[...], wqo[:, :, 0:lanes].reshape(NZ * NY * shard, lanes), preferred_element_type=F32)
    qf[...] = q.astype(BF16).astype(F32) * (HEAD ** -0.5)

    r = lax.broadcasted_iota(jnp.int32, (WINDOW, 2 * WINDOW), 0)
    k_ = lax.broadcasted_iota(jnp.int32, (WINDOW, 2 * WINDOW), 1)
    dist = WINDOW + r - k_
    near = (dist >= 0) & (dist <= WINDOW)
    bias_a[1] = jnp.where(near, 0.0, NEG)
    bias_a[0] = jnp.where(near & ((k_ >= WINDOW) | (sp > 0)), 0.0, NEG)
    r = lax.broadcasted_iota(jnp.int32, (WINDOW, 5 * WINDOW), 0)
    k_ = lax.broadcasted_iota(jnp.int32, (WINDOW, 5 * WINDOW), 1)
    back = lax.shift_right_logical(k_, 7)
    kr = k_ & 127
    db = lax.shift_right_logical(r, 5) - lax.shift_right_logical(kr, 5)
    dist = rows * back + 16 * ((r & 31) - (kr & 31)) + 4 * db
    seen = (dist >= 0) & (back <= sp)
    in16 = seen & (db == 0) & (dist <= 16 * WINDOW)
    in4 = seen & (dist <= 4 * WINDOW)
    bias_b[...] = jnp.where(in16 & in4, LN2, jnp.where(in16 | in4, 0.0, NEG))

    for e in range(4):
        prev_copy(e).wait_recv()
        for k in (1, 3, 2):
            @pl.when(y + k >= NY)
            def _():
                row_copy(e, k, 4).start()

    head0 = lax.broadcasted_iota(jnp.int32, (WINDOW, lanes), 1) < HEAD

    def attend(qb, kb, vb, bias):
        q0 = jnp.where(head0, qb, 0.0).astype(BF16)
        q1 = jnp.where(head0, 0.0, qb).astype(BF16)
        s = nt_dot(jnp.concatenate([q0, q1], 0), kb)
        probs, tops, sums = [], [], []
        for h in range(2):
            sh = s[h * WINDOW:(h + 1) * WINDOW] + bias
            top = jnp.max(sh, axis=1, keepdims=True)
            w = jnp.exp(sh - top)
            tops.append(top)
            sums.append(jnp.sum(w, axis=1, keepdims=True))
            probs.append(w.astype(BF16))
        o = jnp.dot(jnp.concatenate(probs, 0), vb, preferred_element_type=F32)
        out = jnp.where(head0, o[0:WINDOW], o[WINDOW:])
        return out, jnp.where(head0, tops[0], tops[1]), jnp.where(head0, sums[0], sums[1])

    for e in range(4):
        row_copy(e, 1, 0).wait_recv()
    for e in range(4):
        for b in range(4):
            for j in range(2):
                tail = halo[e, 1, 32 * b + 24:32 * b + 32, j * lanes:(j + 1) * lanes]
                kvf[j, pl.ds(4 * b + e, 8, stride=16), :] = tail.astype(F32)
    for i in range(rows // WINDOW):
        span = slice(i * WINDOW, (i + 1) * WINDOW)
        keys = slice(i * WINDOW, (i + 2) * WINDOW)
        out, top, total = attend(
            qf[span, :], kvf[0, keys, :].astype(BF16), kvf[1, keys, :].astype(BF16), bias_a[min(i, 1)]
        )
        oa[span, :] = out
        ma[span, :] = top
        la[span, :] = total

    for k in range(chunks):
        x_relay(k)

    for e in range(4):
        row_copy(e, 3, 0).wait_recv()
        row_copy(e, 2, 0).wait_recv()
        pick = [pl.ds(4 * b + e, 32, stride=16) for b in range(4)]
        qb = jnp.concatenate([qf[p, :] for p in pick], 0)
        kvb = halo[e].reshape(5 * WINDOW, 2 * lanes)
        out, top, total = attend(qb, kvb[:, 0:lanes], kvb[:, lanes:], bias_b[...])
        o_a = jnp.concatenate([oa[p, :] for p in pick], 0)
        m_a = jnp.concatenate([ma[p, :] for p in pick], 0)
        l_a = jnp.concatenate([la[p, :] for p in pick], 0)
        peak = jnp.maximum(top, m_a)
        f_b = jnp.exp(top - peak)
        f_a = jnp.exp(m_a - peak)
        denom = f_a * l_a + f_b * total
        res = (f_a * o_a + f_b * out) / denom
        lse = peak + jnp.log(denom)
        for b in range(4):
            att[pick[b], :] = res[32 * b:32 * b + 32]
            lse_rows[pick[b], :] = lse[32 * b:32 * b + 32]

    att_b[...] = att[...].reshape(NX, rows // NX, lanes).astype(BF16)

    def att_copy(d):
        return remote(att_b.at[at_x(d)], att_x.at[NX - d], as_.at[d - 1], ar.at[d - 1], {"x": at_x(d)})

    for d in (1, 3, 2):
        start(att_copy(d))
    att_x[0] = att_b[x]
    lse_t = lse_rows[...].T
    lse_out[0:1, :] = lse_t[0:1, :]
    lse_out[1:2, :] = lse_t[HEAD:HEAD + 1, :]
    for k in range(chunks):
        x_copy(2 if k < chunks // 2 else 3, k, 0).wait_recv()
    for d in (1, 3, 2):
        att_copy(d).wait_recv()

    groups = 8
    width = NZ * NY // groups
    hrows = rows // NX // 2

    def core_copy(j):
        return remote(part_b.at[j, 1 - c], part_x.at[j], cs.at[j], cr.at[j], {"c": 1 - c})

    for g in range(groups):
        span = slice(g * width, (g + 1) * width)
        w0 = wqo[span, :, lanes:].reshape(width * shard, lanes)
        acc = nt_dot(att_x[0], w0)
        for k in range(1, NX):
            acc += nt_dot(att_x[k], wox[k - 1, span].reshape(width * shard, lanes))
        acc = acc.reshape(2, hrows, width * shard)
        part[g] = acc
        part_b[g] = acc.astype(BF16)
        start(core_copy(g))
    for g in range(groups):
        core_copy(g).wait_recv()
        mixed[:, g * width * shard:(g + 1) * width * shard] = (part[g, c] + part_x[g].astype(F32)).astype(BF16)

    for e in range(4):
        prev_copy(e).wait_send()
        for k in (1, 2, 3):
            row_copy(e, k, 0).wait_send()
    for cp in sends:
        cp.wait_send()


def shards(tokens, w_query, w_key, w_value, w_out):
    rows, depth = tokens.shape
    shard, lanes = w_query.shape
    n_sp = NZ * NY
    groups = 8
    wide = n_sp // groups * shard
    vmem = pl.BlockSpec(memory_space=pltpu.VMEM)
    dma = pltpu.SemaphoreType.DMA
    return pl.pallas_call(
        layer_kernel,
        name="layer",
        out_shape=(
            jax.ShapeDtypeStruct((rows // 8, depth), BF16),
            jax.ShapeDtypeStruct((2, rows), F32),
        ),
        in_specs=[pl.BlockSpec(memory_space=pl.ANY)] + [vmem] * 4,
        out_specs=(vmem, vmem),
        scratch_shapes=[
            pltpu.VMEM((rows, depth), BF16),
            pltpu.VMEM((n_sp, shard, 2 * lanes), BF16),
            pltpu.VMEM((n_sp, shard, 2 * lanes), BF16),
            pltpu.VMEM((NX - 1, n_sp, shard, lanes), BF16),
            pltpu.VMEM((4, 5, WINDOW, 2 * lanes), BF16),
            pltpu.VMEM((rows, lanes), F32),
            pltpu.VMEM((2, WINDOW + rows, lanes), F32),
            pltpu.VMEM((rows, lanes), F32),
            pltpu.VMEM((rows, lanes), F32),
            pltpu.VMEM((rows, lanes), F32),
            pltpu.VMEM((rows, lanes), F32),
            pltpu.VMEM((rows, lanes), F32),
            pltpu.VMEM((NX, rows // NX, lanes), BF16),
            pltpu.VMEM((NX, rows // NX, lanes), BF16),
            pltpu.VMEM((groups, 2, rows // NX // 2, wide), F32),
            pltpu.VMEM((groups, 2, rows // NX // 2, wide), BF16),
            pltpu.VMEM((groups, rows // NX // 2, wide), BF16),
            pltpu.VMEM((2, WINDOW, 2 * WINDOW), F32),
            pltpu.VMEM((WINDOW, 5 * WINDOW), F32),
            dma,
            dma((3,)), dma((3,)),
            dma((2, 2, NZ // 2)), dma((2, 2, NZ // 2)),
            dma((4, NZ)), dma((4, NZ)),
            dma((3, 4)), dma((3, 4)),
            dma((4, 4)), dma((4, 4)),
            dma((3,)), dma((3,)),
            dma((groups,)), dma((groups,)),
        ],
        compiler_params=pltpu.CompilerParams(
            collective_id=0, has_side_effects=True, vmem_limit_bytes=60 * 1024 * 1024
        ),
    )(tokens, w_query, w_key, w_value, w_out.T)


def solution(mesh):
    torus = Mesh(mesh.devices.reshape(NZ, NY, NX, 2), ("z", "y", "x", "c"))
    in_specs = (P(SP, None), P(SP, TP), P(SP, TP), P(SP, TP), P(TP, SP))
    out_specs = (P(SP + TP, None), P(TP, SP))
    return jax.shard_map(
        shards, mesh=torus, in_specs=in_specs, out_specs=out_specs, check_vma=False
    )
```

time: 324 us -> 92.7 us (0.29)
  waiting for transfers between devices: 127 us -> 0 us
  Pallas kernels: 0 us -> 88.8 us
  local copies, waits for them, and re-layouts: 57.8 us -> 3.03 us
  blocking collectives: 47.5 us -> 0 us
  starting transfers between devices: 37.8 us -> 0 us
  other arithmetic: 18.9 us -> 0 us
  matrix products: 18.6 us -> 0 us
  between operations: 14.3 us -> 0.64 us
    all_gather x1 -> x0, waiting for transfers between devices: 90.2 us -> none  [sent_together(): result = lax.all_gather(both, axis, axis=dim, tiled=True)]
    pallas_call x0 -> x1, Pallas kernels: none -> 88.8 us  [shards(): pl.pallas_call(layer_kernel, name='layer', out_shape=(jax.ShapeDtypeStruc...]
    all_gather x2 -> x0, blocking collectives: 47.5 us -> none  [whole_of(): shard = lax.all_gather(shard, axis, axis=dim, tiled=True)]
    all_to_all x1 -> x0, waiting for transfers between devices: 37 us -> none  [summed_on_arrival(): lax.all_to_all(in_blocks(shard, dim, count), axis, 0, 0, tiled=True)]
    reshape x13 -> x0, local copies, waits for them, and re-layouts: 29.8 us -> none  [the longest x4 11.4 us: shards(): value_all_rows.reshape(KEYS_BEHIND + sequence_length, dilation_rate, head...]
    ppermute x6 -> x0, starting transfers between devices: 20.4 us -> none  [passed_along(): return lax.ppermute(block, axis, route)]
    dot_general x10 -> x0, matrix products: 18.6 us -> none  [the longest x3 5.5 us: shards(): jnp.dot(tokens, piece, preferred_element_type=jnp.float32)]
    all_to_all x1 -> x0, starting transfers between devices: 17.3 us -> none  [summed_on_arrival(): lax.all_to_all(in_blocks(shard, dim, count), axis, 0, 0, tiled=True)]
  transfers between devices with their start and end apart: 8 -> 0, of which waited for: 2 -> 0; matrix products, arithmetic and copies ran while one was open for 15% -> 0% of each run, Pallas kernels for 0% -> 0%
where the time goes in v1:
time: 92.7 us; the launch traced here: 92.4 us
  Pallas kernels  88.8 us (96%)
  local copies, waits for them, and re-layouts  3.03 us (3%)
    pallas_call x1, Pallas kernels, shards(): pl.pallas_call(layer_kernel, name='layer', out_shape=(jax.ShapeDtypeStruc...  88.8 us
    unnamed x2, local copies, waits for them, and re-layouts  3.03 us

profile of v1, /device:TPU:1, one launch (start us, length us, event | category | flops | bytes accessed | tf_op | source)
XLA Modules:
  0.0 92.4 jit_solution(5766356355994246627)
XLA Ops:
  0.6 88.8 %layer.1 = (bf16[64,3072]{1,0:T(8,128)(2,1)}, f32[2,512]{1,0:T(2,128)}) custom-call(bf16[512,3072]{1,0:T(8,128)(2,1)} %tokens.1, bf16[48,128]{1,0:T(8,128)(2,1)} %wq.1, bf16[48,128]{1,0:T(8,128)(2,1)} %wk.1, bf16[48,128]{1,0:T(8,128)(2,1)} %wv.1, bf16[48,128]{1,0:T(8,128)(2,1)} %bitcast.1), custom_call_target="tpu_custom_call" | custom-call | tf_op jit(solution)/shard_map/layer/pallas_call | solution.py:339
  89.4 1.8 %copy.9 = bf16[64,3072]{1,0:T(8,128)(2,1)} copy(bf16[64,3072]{1,0:T(8,128)(2,1)} %get-tuple-element.4) | data formatting | bytes 786432
  91.2 1.3 %copy.10 = f32[2,512]{1,0:T(2,128)} copy(f32[2,512]{1,0:T(2,128)} %get-tuple-element.5) | data formatting | bytes 8192

commit v2 on v1

v2 whole, which is shorter than its diff:
```python
import jax
import jax.numpy as jnp
from jax import lax
from jax.experimental import pallas as pl
from jax.experimental.pallas import tpu as pltpu
from jax.sharding import Mesh
from jax.sharding import PartitionSpec as P

HEAD = 64
WINDOW = 128
NZ = 16
NY = 4
NX = 4
MESH = pl.DeviceIdType.MESH
SP = ("z", "y")
TP = ("x", "c")
NEG = -1e30
LN2 = 0.6931471805599453
F32 = jnp.float32
BF16 = jnp.bfloat16
Z_PARTS = [(0, 2), (2, 1)]
LAST_PARTS = [[(0, 2)], [(2, 1)]]
O_PARTS = [(0, 2), (2, 2)]
X_ORDER = [0] + [v for s in range(1, NZ // 2) for v in (s, NZ - s)] + [NZ // 2]


def nt_dot(a, b):
    return lax.dot_general(a, b, (((1,), (1,)), ((), ())), preferred_element_type=F32)


def remote(src, dst, send, recv, device):
    return pltpu.make_async_remote_copy(
        src_ref=src, dst_ref=dst, send_sem=send, recv_sem=recv, device_id=device, device_id_type=MESH
    )


def layer_kernel(
    tokens, wq, wk, wv, wo, mixed, lse_out,
    tok, w3, wox, halo, qf, kvf, oa, ma, la, att, lse_rows, att_b, att_x, part, part_b, part_x,
    bias_a, bias_b,
    load_sem, out_sem, oy_r, zr, or_, yr, yd, xr, xd, hr, ar, cr,
):
    z, y, x, c = (lax.axis_index(n) for n in ("z", "y", "x", "c"))
    sp = z * NY + y
    shard, lanes = wk.shape
    rows = tokens.shape[0]
    loads = [
        pltpu.make_async_copy(wk, w3.at[sp, :, pl.ds(0, lanes)], load_sem.at[1]),
        pltpu.make_async_copy(wv, w3.at[sp, :, pl.ds(lanes, lanes)], load_sem.at[2]),
        pltpu.make_async_copy(wq, w3.at[sp, :, pl.ds(2 * lanes, lanes)], load_sem.at[3]),
        pltpu.make_async_copy(wo, wox.at[0, sp], load_sem.at[4]),
    ]
    for cp in loads:
        cp.start()
    copy_tokens = pltpu.make_async_copy(tokens, tok, load_sem.at[0])
    copy_tokens.start()

    def at_z(d):
        return lax.rem(z + d + NZ, NZ)

    def at_y(d):
        return lax.rem(y + d + NY, NY)

    def at_x(d):
        return lax.rem(x + d + NX, NX)

    barrier = pltpu.get_barrier_semaphore()
    peers = [{"z": at_z(1)}, {"z": at_z(-1)}]
    peers += [{"y": at_y(d)} for d in range(1, NY)]
    peers += [{"x": at_x(d)} for d in range(1, NX)]
    peers += [{"c": 1 - c}]
    for peer in peers:
        pl.semaphore_signal(barrier, inc=1, device_id=peer, device_id_type=MESH)
    for cp in loads:
        cp.wait()
    pl.semaphore_wait(barrier, len(peers))

    z_to = [{"z": at_z(1)}, {"z": at_z(-1)}]
    y_to = [{"y": at_y(1)}, {"y": at_y(-1)}]
    last = NZ // 2

    def z_parts(way, s):
        if s < last:
            return Z_PARTS
        return LAST_PARTS[way]

    def z_copy(way, s, part_):
        src = at_z(-s if way == 0 else s)
        lo, n = part_
        ref = w3.at[src * NY + y, :, pl.ds(lo * lanes, n * lanes)]
        return remote(ref, ref, out_sem.at[0], zr.at[way, s - 1, lo // 2], z_to[way])

    def z_send(way, s, part_):
        src = at_z(-(s - 1) if way == 0 else s - 1)
        lo, n = part_
        ref = w3.at[src * NY + y, :, pl.ds(lo * lanes, n * lanes)]
        remote(ref, ref, out_sem.at[0], zr.at[way, s - 1, lo // 2], z_to[way]).start()

    def o_parts(way, s):
        if s < last:
            return O_PARTS
        return [(2 * way, 2)]

    def o_ref(way, hop, part_):
        src = at_z(-hop if way == 0 else hop)
        lo, n = part_
        return wox.at[0, pl.ds(src * NY + lo, n)]

    def o_copy(way, s, hop, part_):
        ref = o_ref(way, hop, part_)
        lo = part_[0]
        return remote(ref, ref, out_sem.at[1], or_.at[way, s - 1, lo // 2], z_to[way])

    def y_copy(kind, slot, col):
        ref = w3.at[at_z(-slot) * NY + at_y(col)]
        split = (2 - slot % 2) * lanes
        if kind == 2:
            ref = ref.at[:, pl.ds(0, split)]
        if kind == 3:
            ref = ref.at[:, pl.ds(split, 3 * lanes - split)]
        return remote(ref, ref, out_sem.at[2], yr.at[kind, slot] if kind < 2 else yd, y_to[kind % 2])

    def y_send(slot):
        y_copy(0, slot, 0).start()
        y_copy(1, slot, 0).start()

    def y_relay(slot):
        y_copy(0, slot, -1).wait_recv()
        y_copy(2, slot, -1).start()
        y_copy(1, slot, 1).wait_recv()
        y_copy(3, slot, 1).start()

    def arrived_all(ref, sem):
        remote(ref, ref, out_sem.at[0], sem, z_to[0]).wait_recv()

    def left_all(ref, sem):
        remote(ref, ref, sem, yd, z_to[0]).wait_send()

    def x_copy(kind, slot):
        span = pl.ds(at_z(-slot) * NY, NY)
        way = (0, 1, slot % 2)[kind]
        src = wox.at[(0, 0, (NX - 1, 1)[way])[kind], span]
        dst = wox.at[(NX - 1, 1, 2)[kind], span]
        return remote(src, dst, out_sem.at[3], xr.at[kind, X_ORDER.index(slot) // 8] if kind < 2 else xd, {"x": at_x(1 if way == 0 else -1)})

    def x_send(slot):
        x_copy(0, slot).start()
        x_copy(1, slot).start()

    def x_relay(group):
        for kind in (0, 1):
            arrived_all(wox.at[0, pl.ds(0, 8 * NY)], xr.at[kind, group])
        for slot in X_ORDER[8 * group:8 * group + 8]:
            x_copy(2, slot).start()

    def o_row(d, col):
        ref = wox.at[0, z * NY + at_y(col)]
        return remote(ref, ref, out_sem.at[4], oy_r, {"y": at_y(d)})

    for d in (1, 3, 2):
        o_row(d, 0).start()
    for part_ in Z_PARTS:
        for way in (0, 1):
            z_send(way, 1, part_)
    y_send(0)
    arrived_all(wox.at[0, pl.ds(0, NY - 1)], oy_r)
    for part_ in O_PARTS:
        for way in (0, 1):
            o_copy(way, 1, 0, part_).start()
    x_send(0)
    waiting = [0]
    for s in range(1, last + 1):
        for i in range(len(Z_PARTS)):
            for way in (0, 1):
                here = z_parts(way, s)
                if i < len(here):
                    z_copy(way, s, here[i]).wait_recv()
                    if s + 1 < last or (s + 1 == last and here[i] in LAST_PARTS[way]):
                        z_send(way, s + 1, here[i])
        arrived = [s, NZ - s] if s < last else [s]
        for slot in arrived:
            y_send(slot)
        for i in range(len(O_PARTS)):
            for way in (0, 1):
                here = o_parts(way, s)
                if i < len(here):
                    o_copy(way, s, s, here[i]).wait_recv()
                    if s + 1 < last or (s + 1 == last and here[i] in [(2 * way, 2)]):
                        o_copy(way, s + 1, s, here[i]).start()
        for slot in arrived:
            x_send(slot)
        for slot in waiting:
            y_relay(slot)
        waiting = arrived
    for slot in waiting:
        y_relay(slot)
    arrived_all(w3.at[pl.ds(0, NZ)], yd)

    copy_tokens.wait()
    qkv = jnp.dot(tok[...], w3[...].reshape(NZ * NY * shard, 3 * lanes), preferred_element_type=F32)
    for j in range(2):
        side = slice(j * lanes, (j + 1) * lanes)
        kvf[j, WINDOW:, :] = qkv[:, side]
        for e in range(4):
            for b in range(4):
                picked = kvf[j, pl.ds(WINDOW + 4 * b + e, 32, stride=16), :]
                halo[e, 0, 32 * b:32 * b + 32, side] = picked.astype(BF16)
    qf[...] = qkv[:, 2 * lanes:].astype(BF16).astype(F32) * (HEAD ** -0.5)
    def prev_copy(e):
        return remote(halo.at[e, 0], halo.at[e, 4], out_sem.at[5], hr.at[0, e], z_to[0])

    def row_copy(e, k, src):
        return remote(halo.at[e, src], halo.at[e, k], out_sem.at[5], hr.at[k, e], {"y": at_y(k)})

    for e in range(4):
        prev_copy(e).start()
    for k in (1, 3, 2):
        @pl.when(y + k < NY)
        def _():
            for e in range(4):
                row_copy(e, k, 0).start()

    r = lax.broadcasted_iota(jnp.int32, (WINDOW, 2 * WINDOW), 0)
    k_ = lax.broadcasted_iota(jnp.int32, (WINDOW, 2 * WINDOW), 1)
    dist = WINDOW + r - k_
    near = (dist >= 0) & (dist <= WINDOW)
    bias_a[1] = jnp.where(near, 0.0, NEG)
    bias_a[0] = jnp.where(near & ((k_ >= WINDOW) | (sp > 0)), 0.0, NEG)
    r = lax.broadcasted_iota(jnp.int32, (WINDOW, 5 * WINDOW), 0)
    k_ = lax.broadcasted_iota(jnp.int32, (WINDOW, 5 * WINDOW), 1)
    back = lax.shift_right_logical(k_, 7)
    kr = k_ & 127
    db = lax.shift_right_logical(r, 5) - lax.shift_right_logical(kr, 5)
    dist = rows * back + 16 * ((r & 31) - (kr & 31)) + 4 * db
    seen = (dist >= 0) & (back <= sp)
    in16 = seen & (db == 0) & (dist <= 16 * WINDOW)
    in4 = seen & (dist <= 4 * WINDOW)
    bias_b[...] = jnp.where(in16 & in4, LN2, jnp.where(in16 | in4, 0.0, NEG))

    x_relay(0)
    for e in range(4):
        prev_copy(e).wait_recv()
        for k in (1, 3, 2):
            @pl.when(y + k >= NY)
            def _():
                row_copy(e, k, 4).start()

    head0 = lax.broadcasted_iota(jnp.int32, (WINDOW, lanes), 1) < HEAD

    def attend(qb, kb, vb, bias):
        q0 = jnp.where(head0, qb, 0.0).astype(BF16)
        q1 = jnp.where(head0, 0.0, qb).astype(BF16)
        s = nt_dot(jnp.concatenate([q0, q1], 0), kb)
        probs, tops, sums = [], [], []
        for h in range(2):
            sh = s[h * WINDOW:(h + 1) * WINDOW] + bias
            top = jnp.max(sh, axis=1, keepdims=True)
            w = jnp.exp(sh - top)
            tops.append(top)
            sums.append(jnp.sum(w, axis=1, keepdims=True))
            probs.append(w.astype(BF16))
        o = jnp.dot(jnp.concatenate(probs, 0), vb, preferred_element_type=F32)
        out = jnp.where(head0, o[0:WINDOW], o[WINDOW:])
        return out, jnp.where(head0, tops[0], tops[1]), jnp.where(head0, sums[0], sums[1])

    for e in range(4):
        row_copy(e, 1, 0).wait_recv()
    for e in range(4):
        for b in range(4):
            for j in range(2):
                tail = halo[e, 1, 32 * b + 24:32 * b + 32, j * lanes:(j + 1) * lanes]
                kvf[j, pl.ds(4 * b + e, 8, stride=16), :] = tail.astype(F32)
    for i in range(rows // WINDOW):
        span = slice(i * WINDOW, (i + 1) * WINDOW)
        keys = slice(i * WINDOW, (i + 2) * WINDOW)
        out, top, total = attend(
            qf[span, :], kvf[0, keys, :].astype(BF16), kvf[1, keys, :].astype(BF16), bias_a[min(i, 1)]
        )
        oa[span, :] = out
        ma[span, :] = top
        la[span, :] = total

    x_relay(1)

    for e in range(4):
        row_copy(e, 3, 0).wait_recv()
        row_copy(e, 2, 0).wait_recv()
        pick = [pl.ds(4 * b + e, 32, stride=16) for b in range(4)]
        qb = jnp.concatenate([qf[p, :] for p in pick], 0)
        kvb = halo[e].reshape(5 * WINDOW, 2 * lanes)
        out, top, total = attend(qb, kvb[:, 0:lanes], kvb[:, lanes:], bias_b[...])
        o_a = jnp.concatenate([oa[p, :] for p in pick], 0)
        m_a = jnp.concatenate([ma[p, :] for p in pick], 0)
        l_a = jnp.concatenate([la[p, :] for p in pick], 0)
        peak = jnp.maximum(top, m_a)
        f_b = jnp.exp(top - peak)
        f_a = jnp.exp(m_a - peak)
        denom = f_a * l_a + f_b * total
        res = (f_a * o_a + f_b * out) / denom
        lse = peak + jnp.log(denom)
        for b in range(4):
            att[pick[b], :] = res[32 * b:32 * b + 32]
            lse_rows[pick[b], :] = lse[32 * b:32 * b + 32]

    att_b[...] = att[...].reshape(NX, rows // NX, lanes).astype(BF16)

    def att_copy(d):
        return remote(att_b.at[at_x(d)], att_x.at[NX - d], out_sem.at[6], ar, {"x": at_x(d)})

    for d in (1, 3, 2):
        att_copy(d).start()
    att_x[0] = att_b[x]
    lse_t = lse_rows[...].T
    lse_out[0:1, :] = lse_t[0:1, :]
    lse_out[1:2, :] = lse_t[HEAD:HEAD + 1, :]
    arrived_all(wox.at[2], xd)
    arrived_all(att_x.at[pl.ds(1, NX - 1)], ar)

    groups = 8
    width = NZ * NY // groups
    hrows = rows // NX // 2

    def core_copy(j):
        return remote(part_b.at[j, 1 - c], part_x.at[j], out_sem.at[7], cr.at[j], {"c": 1 - c})

    for g in range(groups):
        span = slice(g * width, (g + 1) * width)
        acc = nt_dot(att_x[0], wox[0, span].reshape(width * shard, lanes))
        for k in range(1, NX):
            acc += nt_dot(att_x[k], wox[k, span].reshape(width * shard, lanes))
        acc = acc.reshape(2, hrows, width * shard)
        part[g] = acc
        part_b[g] = acc.astype(BF16)
        core_copy(g).start()
    for g in range(groups):
        core_copy(g).wait_recv()
        mixed[:, g * width * shard:(g + 1) * width * shard] = (part[g, c] + part_x[g].astype(F32)).astype(BF16)

    left_all(w3.at[pl.ds(0, NZ - 1)], out_sem.at[0])
    left_all(wox.at[0, pl.ds(0, (NZ - 1) * NY)], out_sem.at[1])
    left_all(w3.at[pl.ds(0, 3 * NZ)], out_sem.at[2])
    left_all(wox.at[pl.ds(0, NX - 1)], out_sem.at[3])
    left_all(wox.at[0, pl.ds(0, NY - 1)], out_sem.at[4])
    left_all(halo.at[:, pl.ds(0, 4)], out_sem.at[5])
    left_all(att_x.at[pl.ds(1, NX - 1)], out_sem.at[6])
    left_all(part_x, out_sem.at[7])


def shards(tokens, w_query, w_key, w_value, w_out):
    rows, depth = tokens.shape
    shard, lanes = w_query.shape
    n_sp = NZ * NY
    groups = 8
    wide = n_sp // groups * shard
    vmem = pl.BlockSpec(memory_space=pltpu.VMEM)
    dma = pltpu.SemaphoreType.DMA
    return pl.pallas_call(
        layer_kernel,
        name="layer",
        out_shape=(
            jax.ShapeDtypeStruct((rows // 8, depth), BF16),
            jax.ShapeDtypeStruct((2, rows), F32),
        ),
        in_specs=[pl.BlockSpec(memory_space=pl.ANY)] * 5,
        out_specs=(vmem, vmem),
        scratch_shapes=[
            pltpu.VMEM((rows, depth), BF16),
            pltpu.VMEM((n_sp, shard, 3 * lanes), BF16),
            pltpu.VMEM((NX, n_sp, shard, lanes), BF16),
            pltpu.VMEM((4, 5, WINDOW, 2 * lanes), BF16),
            pltpu.VMEM((rows, lanes), F32),
            pltpu.VMEM((2, WINDOW + rows, lanes), F32),
            pltpu.VMEM((rows, lanes), F32),
            pltpu.VMEM((rows, lanes), F32),
            pltpu.VMEM((rows, lanes), F32),
            pltpu.VMEM((rows, lanes), F32),
            pltpu.VMEM((rows, lanes), F32),
            pltpu.VMEM((NX, rows // NX, lanes), BF16),
            pltpu.VMEM((NX, rows // NX, lanes), BF16),
            pltpu.VMEM((groups, 2, rows // NX // 2, wide), F32),
            pltpu.VMEM((groups, 2, rows // NX // 2, wide), BF16),
            pltpu.VMEM((groups, rows // NX // 2, wide), BF16),
            pltpu.VMEM((2, WINDOW, 2 * WINDOW), F32),
            pltpu.VMEM((WINDOW, 5 * WINDOW), F32),
            dma((5,)),
            dma((8,)),
            dma,
            dma((2, NZ // 2, 2)),
            dma((2, NZ // 2, 2)),
            dma((2, NZ)),
            dma,
            dma((2, 2)),
            dma,
            dma((4, 4)),
            dma,
            dma((groups,)),
        ],
        compiler_params=pltpu.CompilerParams(
            collective_id=0, has_side_effects=True, vmem_limit_bytes=60 * 1024 * 1024
        ),
    )(tokens, w_query, w_key, w_value, w_out.T)


def solution(mesh):
    torus = Mesh(mesh.devices.reshape(NZ, NY, NX, 2), ("z", "y", "x", "c"))
    in_specs = (P(SP, None), P(SP, TP), P(SP, TP), P(SP, TP), P(TP, SP))
    out_specs = (P(SP + TP, None), P(TP, SP))
    return jax.shard_map(
        shards, mesh=torus, in_specs=in_specs, out_specs=out_specs, check_vma=False
    )
```

time: 92.7 us -> 79.9 us (0.86)
  Pallas kernels: 88.8 us -> 76 us
    pallas_call x1, Pallas kernels: 88.8 us -> 76 us  [shards(): pl.pallas_call(layer_kernel, name='layer', out_shape=(jax.ShapeDtypeStruc...]
where the time goes in v2:
time: 79.9 us; the launch traced here: 79.7 us
  Pallas kernels  76 us (95%)
  local copies, waits for them, and re-layouts  3.03 us (4%)
    pallas_call x1, Pallas kernels, shards(): pl.pallas_call(layer_kernel, name='layer', out_shape=(jax.ShapeDtypeStruc...  76 us
    unnamed x2, local copies, waits for them, and re-layouts  3.03 us

profile of v2, /device:TPU:1, one launch (start us, length us, event | category | flops | bytes accessed | tf_op | source)
XLA Modules:
  0.0 79.7 jit_solution(14876579450183384972)
XLA Ops:
  0.6 76.0 %layer.1 = (bf16[64,3072]{1,0:T(8,128)(2,1)}, f32[2,512]{1,0:T(2,128)}) custom-call(bf16[512,3072]{1,0:T(8,128)(2,1)} %tokens.1, bf16[48,128]{1,0:T(8,128)(2,1)} %wq.1, bf16[48,128]{1,0:T(8,128)(2,1)} %wk.1, bf16[48,128]{1,0:T(8,128)(2,1)} %wv.1, bf16[48,128]{1,0:T(8,128)(2,1)} %bitcast.1), custom_call_target="tpu_custom_call" | custom-call | tf_op jit(solution)/shard_map/layer/pallas_call | solution.py:357
  76.7 1.8 %copy.9 = bf16[64,3072]{1,0:T(8,128)(2,1)} copy(bf16[64,3072]{1,0:T(8,128)(2,1)} %get-tuple-element.4) | data formatting | bytes 786432
  78.4 1.3 %copy.10 = f32[2,512]{1,0:T(2,128)} copy(f32[2,512]{1,0:T(2,128)} %get-tuple-element.5) | data formatting | bytes 8192

commit v3 on v1

v3 whole, which is shorter than its diff:
```python
import jax
import jax.numpy as jnp
from jax import lax
from jax.experimental import pallas as pl
from jax.experimental.pallas import tpu as pltpu
from jax.sharding import Mesh
from jax.sharding import PartitionSpec as P

HEAD = 64
WINDOW = 128
NZ = 16
NY = 4
NX = 4
MESH = pl.DeviceIdType.MESH
SP = ("z", "y")
TP = ("x", "c")
NEG = -1e30
LN2 = 0.6931471805599453
F32 = jnp.float32
BF16 = jnp.bfloat16
X_ORDER = [0] + [v for s in range(1, NZ // 2) for v in (s, NZ - s)] + [NZ // 2]


Q_LAG = 4
DIRECT = (NZ // 2 - 1, NZ // 2, NZ // 2 + 1)


def nt_dot(a, b):
    return lax.dot_general(a, b, (((1,), (1,)), ((), ())), preferred_element_type=F32)


def remote(src, dst, send, recv, device):
    return pltpu.make_async_remote_copy(
        src_ref=src, dst_ref=dst, send_sem=send, recv_sem=recv, device_id=device, device_id_type=MESH
    )


def layer_kernel(
    tokens, wq, wk_in, wv, wo, mixed, lse_out,
    tok, wz, wog, wox, halo, qf, kvf, oa, ma, la, att, lse_rows, att_b, att_x, part, part_b, part_x,
    bias_a, bias_b,
    load_sem, out_sem, row_r, zr, yr, yd, push_r, o_r, xr, xd, hr, ar, cr,
):
    z, y, x, c = (lax.axis_index(n) for n in ("z", "y", "x", "c"))
    sp = z * NY + y
    shard, lanes = wk_in.shape
    rows = tokens.shape[0]
    other = pl.ds(0, 2 * lanes)
    mine = pl.ds(2 * lanes, 2 * lanes)

    def load(src, dst, k):
        return pltpu.make_async_copy(src, dst, load_sem.at[k])

    def loads(first):
        lo, slot = (0, 1) if first else (2 * lanes, 0)
        return [
            load(wk_in, wz.at[sp, :, pl.ds(lo, lanes)], 1),
            load(wv, wz.at[sp, :, pl.ds(lo + lanes, lanes)], 2),
            load(wo, wog.at[slot, sp], 3),
            load(wq, wog.at[slot + 2, sp], 4),
        ]

    for core in (0, 1):
        @pl.when(c == core)
        def _():
            for cp in loads(core == 0):
                cp.start()
    copy_tokens = load(tokens, tok, 0)
    copy_tokens.start()

    def at_z(d):
        return lax.rem(z + d + NZ, NZ)

    def at_y(d):
        return lax.rem(y + d + NY, NY)

    def at_x(d):
        return lax.rem(x + d + NX, NX)

    barrier = pltpu.get_barrier_semaphore()
    peers = [{"z": at_z(1)}, {"z": at_z(-1)}]
    peers += [{"y": at_y(d)} for d in range(1, NY)]
    peers += [{"x": at_x(d)} for d in range(1, NX)]
    peers += [{"c": 1 - c}]
    for peer in peers:
        pl.semaphore_signal(barrier, inc=1, device_id=peer, device_id_type=MESH)
    r = lax.broadcasted_iota(jnp.int32, (WINDOW, 2 * WINDOW), 0)
    k_ = lax.broadcasted_iota(jnp.int32, (WINDOW, 2 * WINDOW), 1)
    dist = WINDOW + r - k_
    near = (dist >= 0) & (dist <= WINDOW)
    bias_a[1] = jnp.where(near, 0.0, NEG)
    bias_a[0] = jnp.where(near & ((k_ >= WINDOW) | (sp > 0)), 0.0, NEG)
    r = lax.broadcasted_iota(jnp.int32, (WINDOW, 5 * WINDOW), 0)
    k_ = lax.broadcasted_iota(jnp.int32, (WINDOW, 5 * WINDOW), 1)
    back = lax.shift_right_logical(k_, 7)
    kr = k_ & 127
    db = lax.shift_right_logical(r, 5) - lax.shift_right_logical(kr, 5)
    dist = rows * back + 16 * ((r & 31) - (kr & 31)) + 4 * db
    seen = (dist >= 0) & (back <= sp)
    in16 = seen & (db == 0) & (dist <= 16 * WINDOW)
    in4 = seen & (dist <= 4 * WINDOW)
    bias_b[...] = jnp.where(in16 & in4, LN2, jnp.where(in16 | in4, 0.0, NEG))

    for cp in loads(True):
        cp.wait()
    pl.semaphore_wait(barrier, len(peers))

    z_to = [{"z": at_z(1)}, {"z": at_z(-1)}]
    y_to = [{"y": at_y(1)}, {"y": at_y(-1)}]
    partner = {"c": 1 - c}
    last = NZ // 2

    def arrived_all(ref, sem):
        remote(ref, ref, out_sem.at[0], sem, z_to[0]).wait_recv()

    def left_all(ref, sem):
        remote(ref, ref, sem, xd, z_to[0]).wait_send()

    def z_ref(flow, src, way, s):
        if flow < 2:
            lo, n = (2 * flow, 2) if s < last else (2 * flow + way, 1)
            return wz.at[src * NY + y, :, pl.ds(lo * lanes, n * lanes)]
        cols = pl.ds(src * NY, NY) if s < last else pl.ds(src * NY + 2 * way, 2)
        return wog.at[flow - 2, cols]

    def z_copy(flow, way, s, hop):
        ref = z_ref(flow, at_z(-hop if way == 0 else hop), way, s)
        return remote(ref, ref, out_sem.at[flow // 2], zr.at[flow, way, s - 1], z_to[way])

    def z_first(flow):
        for way in (0, 1):
            z_copy(flow, way, 1, 0).start()

    def z_hop(flow, s):
        for way in (0, 1):
            z_copy(flow, way, s, s).wait_recv()
            if s < last:
                z_copy(flow, way, s + 1, s).start()

    def y_copy(kind, slot, col):
        ref = wz.at[at_z(-slot) * NY + at_y(col)]
        split = 2 * lanes
        if kind == 2:
            ref = ref.at[:, pl.ds(0, split)]
        if kind == 3:
            ref = ref.at[:, pl.ds(split, 2 * lanes)]
        to = {"y": at_y(2)} if kind == 4 else y_to[kind % 2]
        return remote(ref, ref, out_sem.at[3], yr.at[kind, slot] if kind < 2 else yd.at[slot], to)

    def y_send(slot):
        y_copy(0, slot, 0).start()
        y_copy(1, slot, 0).start()
        if slot in DIRECT:
            y_copy(4, slot, 0).start()

    def y_relay(slot):
        y_copy(0, slot, -1).wait_recv()
        if slot not in DIRECT:
            y_copy(2, slot, -1).start()
        y_copy(1, slot, 1).wait_recv()
        if slot not in DIRECT:
            y_copy(3, slot, 1).start()

    def y_done(slot):
        y_copy(4, slot, 2).wait_recv()
        row = pl.ds(at_z(-slot) * NY, NY)
        remote(wz.at[row, :, other], wz.at[row, :, mine], out_sem.at[4], push_r.at[0], partner).start()

    def o_push(slot):
        row = pl.ds(at_z(-slot) * NY, NY)
        group = X_ORDER.index(slot) // 4
        remote(wog.at[1, row], wog.at[0, row], out_sem.at[5], o_r.at[group], partner).start()

    def q_push(slot):
        row = pl.ds(at_z(-slot) * NY, NY)
        remote(wog.at[3, row], wog.at[2, row], out_sem.at[6], push_r.at[1], partner).start()

    def q_hop(s):
        for flow in (4, 5):
            z_hop(flow, s)
        for slot in arrived(s):
            q_push(slot)

    def arrived(s):
        if s == 0:
            return [0]
        return [s, NZ - s] if s < last else [s]

    def x_copy(kind, slot):
        span = pl.ds(at_z(-slot) * NY, NY)
        way = (0, 1, slot % 2)[kind]
        src = wox.at[(2, 0)[way], span] if kind == 2 else wog.at[0, span]
        dst = wox.at[(2, 0, 1)[kind], span]
        return remote(
            src, dst, out_sem.at[7], xr.at[kind, X_ORDER.index(slot) // 8] if kind < 2 else xd,
            {"x": at_x(1 if way == 0 else -1)},
        )

    def x_send(slot):
        x_copy(0, slot).start()
        x_copy(1, slot).start()

    def x_relay(group):
        for kind in (0, 1):
            arrived_all(wox.at[0, pl.ds(0, 8 * NY)], xr.at[kind, group])
        for slot in X_ORDER[8 * group:8 * group + 8]:
            x_copy(2, slot).start()

    def row_send(item, d):
        ref = wog.at[item, sp]
        return remote(ref, ref, out_sem.at[8], row_r.at[item], {"y": at_y(d)})

    @pl.when(c == 0)
    def _():
        remote(wog.at[1, sp], wog.at[1, sp], out_sem.at[1], push_r.at[1], partner).start()
        remote(wz.at[sp, :, other], wz.at[sp, :, other], out_sem.at[0], push_r.at[0], partner).start()
        remote(wog.at[3, sp], wog.at[3, sp], out_sem.at[2], push_r.at[2], partner).start()
        for group in range(4):
            arrived_all(wog.at[0, pl.ds(0, 4 * NY)], o_r.at[group])
            for slot in X_ORDER[4 * group:4 * group + 4]:
                x_send(slot)
        arrived_all(wz.at[:, :, mine], push_r.at[0])

    @pl.when(c == 1)
    def _():
        z_first(1)
        for d in (1, 3, 2):
            row_send(0, d).start()
        arrived_all(wog.at[1, sp], push_r.at[1])
        for d in (1, 3, 2):
            row_send(1, d).start()
        arrived_all(wz.at[sp, :, other], push_r.at[0])
        z_first(0)
        y_send(0)
        arrived_all(wog.at[3, sp], push_r.at[2])
        for item in (2, 3):
            for d in (1, 3, 2):
                row_send(item, d).start()
        for s in range(1, last + 2):
            if s <= last:
                for flow in (1, 0):
                    z_hop(flow, s)
                for slot in arrived(s):
                    y_send(slot)
            for item in (0, 1):
                if s == 1:
                    arrived_all(wog.at[0, pl.ds(0, NY - 1)], row_r.at[item])
                    z_first(2 + item)
                else:
                    z_hop(2 + item, s - 1)
            for slot in arrived(s - 1):
                x_send(slot)
                o_push(slot)
            if s == Q_LAG:
                for item in (2, 3):
                    arrived_all(wog.at[0, pl.ds(0, NY - 1)], row_r.at[item])
                    z_first(2 + item)
                q_push(0)
            if s > Q_LAG:
                q_hop(s - Q_LAG)
            for slot in arrived(s - 1):
                y_relay(slot)
            if s > 1:
                for slot in arrived(s - 2):
                    y_done(slot)
        for slot in arrived(last):
            y_done(slot)

    copy_tokens.wait()
    depth = NZ * NY * shard
    kv = jnp.dot(tok[...], wz[:, :, 2 * lanes:].reshape(depth, 2 * lanes), preferred_element_type=F32)
    for j in range(2):
        side = slice(j * lanes, (j + 1) * lanes)
        kvf[j, WINDOW:, :] = kv[:, side]
        for e in range(4):
            for b in range(4):
                picked = kvf[j, pl.ds(WINDOW + 4 * b + e, 32, stride=16), :]
                halo[e, 0, 32 * b:32 * b + 32, side] = picked.astype(BF16)

    def prev_copy(e):
        return remote(halo.at[e, 0], halo.at[e, 4], out_sem.at[9], hr.at[0, e], z_to[0])

    def row_copy(e, k, src):
        return remote(halo.at[e, src], halo.at[e, k], out_sem.at[9], hr.at[k, e], {"y": at_y(k)})

    def relay_copy(e, k):
        return remote(halo.at[e, k], halo.at[e, 2], out_sem.at[12], hr.at[2, e], y_to[0 if k == 1 else 1])

    def q_next(s):
        @pl.when(c == 1)
        def _():
            q_hop(s)

    for e in range(4):
        prev_copy(e).start()
        for k in (1, 3):
            @pl.when(y + k < NY)
            def _():
                row_copy(e, k, 0).start()

    def wrap(e):
        prev_copy(e).wait_recv()
        for k in (1, 3):
            @pl.when(y + k >= NY)
            def _():
                row_copy(e, k, 4).start()

    def pass_on(e):
        row_copy(e, 1, 0).wait_recv()

        @pl.when((y == 2) | ((y < 2) & (e < 2)))
        def _():
            relay_copy(e, 1).start()

        row_copy(e, 3, 0).wait_recv()

        @pl.when((y == 1) | ((y >= 2) & (e >= 2)))
        def _():
            relay_copy(e, 3).start()

    done = last + 1 - Q_LAG
    q_next(done + 1)
    wrap(0)
    wrap(1)
    for s in range(done + 2, last):
        q_next(s)
    wrap(2)
    wrap(3)
    q_next(last)
    x_relay(0)
    pass_on(0)
    pass_on(1)

    @pl.when(c == 0)
    def _():
        arrived_all(wog.at[2], push_r.at[1])

    q = jnp.dot(tok[...], wog[2].reshape(depth, lanes), preferred_element_type=F32)
    qf[...] = q.astype(BF16).astype(F32) * (HEAD ** -0.5)
    pass_on(2)
    pass_on(3)

    head0 = lax.broadcasted_iota(jnp.int32, (WINDOW, lanes), 1) < HEAD

    def attend(qb, kb, vb, bias):
        q0 = jnp.where(head0, qb, 0.0).astype(BF16)
        q1 = jnp.where(head0, 0.0, qb).astype(BF16)
        s = nt_dot(jnp.concatenate([q0, q1], 0), kb)
        probs, tops, sums = [], [], []
        for h in range(2):
            sh = s[h * WINDOW:(h + 1) * WINDOW] + bias
            top = jnp.max(sh, axis=1, keepdims=True)
            w = jnp.exp(sh - top)
            tops.append(top)
            sums.append(jnp.sum(w, axis=1, keepdims=True))
            probs.append(w.astype(BF16))
        o = jnp.dot(jnp.concatenate(probs, 0), vb, preferred_element_type=F32)
        out = jnp.where(head0, o[0:WINDOW], o[WINDOW:])
        return out, jnp.where(head0, tops[0], tops[1]), jnp.where(head0, sums[0], sums[1])

    for e in range(4):
        for b in range(4):
            for j in range(2):
                tail = halo[e, 1, 32 * b + 24:32 * b + 32, j * lanes:(j + 1) * lanes]
                kvf[j, pl.ds(4 * b + e, 8, stride=16), :] = tail.astype(F32)
    for i in range(rows // WINDOW):
        span = slice(i * WINDOW, (i + 1) * WINDOW)
        keys = slice(i * WINDOW, (i + 2) * WINDOW)
        out, top, total = attend(
            qf[span, :], kvf[0, keys, :].astype(BF16), kvf[1, keys, :].astype(BF16), bias_a[min(i, 1)]
        )
        oa[span, :] = out
        ma[span, :] = top
        la[span, :] = total

    x_relay(1)

    for e in range(4):
        row_copy(e, 2, 0).wait_recv()
        pick = [pl.ds(4 * b + e, 32, stride=16) for b in range(4)]
        qb = jnp.concatenate([qf[p, :] for p in pick], 0)
        kvb = halo[e].reshape(5 * WINDOW, 2 * lanes)
        out, top, total = attend(qb, kvb[:, 0:lanes], kvb[:, lanes:], bias_b[...])
        o_a = jnp.concatenate([oa[p, :] for p in pick], 0)
        m_a = jnp.concatenate([ma[p, :] for p in pick], 0)
        l_a = jnp.concatenate([la[p, :] for p in pick], 0)
        peak = jnp.maximum(top, m_a)
        f_b = jnp.exp(top - peak)
        f_a = jnp.exp(m_a - peak)
        denom = f_a * l_a + f_b * total
        res = (f_a * o_a + f_b * out) / denom
        lse = peak + jnp.log(denom)
        for b in range(4):
            att[pick[b], :] = res[32 * b:32 * b + 32]
            lse_rows[pick[b], :] = lse[32 * b:32 * b + 32]

    att_b[...] = att[...].reshape(NX, rows // NX, lanes).astype(BF16)

    def att_copy(d):
        return remote(att_b.at[at_x(d)], att_x.at[NX - d], out_sem.at[10], ar, {"x": at_x(d)})

    for d in (1, 3, 2):
        att_copy(d).start()
    att_x[0] = att_b[x]
    lse_t = lse_rows[...].T
    lse_out[0:1, :] = lse_t[0:1, :]
    lse_out[1:2, :] = lse_t[HEAD:HEAD + 1, :]
    arrived_all(wox.at[1], xd)
    arrived_all(att_x.at[pl.ds(1, NX - 1)], ar)

    groups = 8
    width = NZ * NY // groups
    hrows = rows // NX // 2

    def core_copy(j):
        return remote(part_b.at[j, 1 - c], part_x.at[j], out_sem.at[11], cr.at[j], {"c": 1 - c})

    for g in range(groups):
        span = slice(g * width, (g + 1) * width)
        acc = nt_dot(att_x[0], wog[0, span].reshape(width * shard, lanes))
        for k in range(1, NX):
            acc += nt_dot(att_x[k], wox[k - 1, span].reshape(width * shard, lanes))
        acc = acc.reshape(2, hrows, width * shard)
        part[g] = acc
        part_b[g] = acc.astype(BF16)
        core_copy(g).start()
    for g in range(groups):
        core_copy(g).wait_recv()
        mixed[:, g * width * shard:(g + 1) * width * shard] = (part[g, c] + part_x[g].astype(F32)).astype(BF16)

    @pl.when(c == 0)
    def _():
        left_all(wz.at[sp, :, other], out_sem.at[0])
        left_all(wog.at[1, sp], out_sem.at[1])
        left_all(wog.at[3, sp], out_sem.at[2])

    @pl.when(c == 1)
    def _():
        left_all(wz.at[pl.ds(0, NZ - 1)], out_sem.at[0])
        for k in (1, 2):
            left_all(wog.at[pl.ds(0, 2), pl.ds(0, (NZ - 1) * NY)], out_sem.at[k])
        left_all(wz.at[pl.ds(0, 3 * NZ)], out_sem.at[3])
        left_all(wz.at[:, :, mine], out_sem.at[4])
        for k in (5, 6):
            left_all(wog.at[0], out_sem.at[k])
        left_all(wog.at[:, pl.ds(0, NY - 1)], out_sem.at[8])

    left_all(wox, out_sem.at[7])
    left_all(halo.at[:, pl.ds(0, 3)], out_sem.at[9])
    left_all(halo.at[0, pl.ds(0, 2)], out_sem.at[12])

    @pl.when((y == 1) | (y == 2))
    def _():
        left_all(halo.at[:, 0], out_sem.at[12])

    left_all(att_x.at[pl.ds(1, NX - 1)], out_sem.at[10])
    left_all(part_x, out_sem.at[11])


def shards(tokens, w_query, w_key, w_value, w_out):
    rows, depth = tokens.shape
    shard, lanes = w_query.shape
    n_sp = NZ * NY
    groups = 8
    wide = n_sp // groups * shard
    vmem = pl.BlockSpec(memory_space=pltpu.VMEM)
    dma = pltpu.SemaphoreType.DMA
    return pl.pallas_call(
        layer_kernel,
        name="layer",
        out_shape=(
            jax.ShapeDtypeStruct((rows // 8, depth), BF16),
            jax.ShapeDtypeStruct((2, rows), F32),
        ),
        in_specs=[pl.BlockSpec(memory_space=pl.ANY)] * 5,
        out_specs=(vmem, vmem),
        scratch_shapes=[
            pltpu.VMEM((rows, depth), BF16),
            pltpu.VMEM((n_sp, shard, 4 * lanes), BF16),
            pltpu.VMEM((4, n_sp, shard, lanes), BF16),
            pltpu.VMEM((NX - 1, n_sp, shard, lanes), BF16),
            pltpu.VMEM((4, 5, WINDOW, 2 * lanes), BF16),
            pltpu.VMEM((rows, lanes), F32),
            pltpu.VMEM((2, WINDOW + rows, lanes), F32),
            pltpu.VMEM((rows, lanes), F32),
            pltpu.VMEM((rows, lanes), F32),
            pltpu.VMEM((rows, lanes), F32),
            pltpu.VMEM((rows, lanes), F32),
            pltpu.VMEM((rows, lanes), F32),
            pltpu.VMEM((NX, rows // NX, lanes), BF16),
            pltpu.VMEM((NX, rows // NX, lanes), BF16),
            pltpu.VMEM((groups, 2, rows // NX // 2, wide), F32),
            pltpu.VMEM((groups, 2, rows // NX // 2, wide), BF16),
            pltpu.VMEM((groups, rows // NX // 2, wide), BF16),
            pltpu.VMEM((2, WINDOW, 2 * WINDOW), F32),
            pltpu.VMEM((WINDOW, 5 * WINDOW), F32),
            dma((5,)),
            dma((13,)),
            dma((4,)),
            dma((6, 2, NZ // 2)),
            dma((2, NZ)),
            dma((NZ,)),
            dma((3,)),
            dma((4,)),
            dma((2, 2)),
            dma,
            dma((4, 4)),
            dma,
            dma((groups,)),
        ],
        compiler_params=pltpu.CompilerParams(
            collective_id=0, has_side_effects=True, vmem_limit_bytes=60 * 1024 * 1024
        ),
    )(tokens, w_query, w_key, w_value, w_out.T)


def solution(mesh):
    torus = Mesh(mesh.devices.reshape(NZ, NY, NX, 2), ("z", "y", "x", "c"))
    in_specs = (P(SP, None), P(SP, TP), P(SP, TP), P(SP, TP), P(TP, SP))
    out_specs = (P(SP + TP, None), P(TP, SP))
    return jax.shard_map(
        shards, mesh=torus, in_specs=in_specs, out_specs=out_specs, check_vma=False
    )
```

time: 92.7 us -> 76.4 us (0.82)
  Pallas kernels: 88.8 us -> 72.5 us
    pallas_call x1, Pallas kernels: 88.8 us -> 72.5 us  [shards(): pl.pallas_call(layer_kernel, name='layer', out_shape=(jax.ShapeDtypeStruc...]
where the time goes in v3:
time: 76.4 us; the launch traced here: 76.2 us
  Pallas kernels  72.5 us (95%)
  local copies, waits for them, and re-layouts  3.03 us (4%)
    pallas_call x1, Pallas kernels, shards(): pl.pallas_call(layer_kernel, name='layer', out_shape=(jax.ShapeDtypeStruc...  72.5 us
    unnamed x2, local copies, waits for them, and re-layouts  3.03 us

profile of v3, /device:TPU:1, one launch (start us, length us, event | category | flops | bytes accessed | tf_op | source)
XLA Modules:
  0.0 76.2 jit_solution(1598490005914394770)
XLA Ops:
  0.6 72.5 %layer.1 = (bf16[64,3072]{1,0:T(8,128)(2,1)}, f32[2,512]{1,0:T(2,128)}) custom-call(bf16[512,3072]{1,0:T(8,128)(2,1)} %tokens.1, bf16[48,128]{1,0:T(8,128)(2,1)} %wq.1, bf16[48,128]{1,0:T(8,128)(2,1)} %wk_in.1, bf16[48,128]{1,0:T(8,128)(2,1)} %wv.1, bf16[48,128]{1,0:T(8,128)(2,1)} %bitcast.1), custom_call_target="tpu_custom_call" | custom-call | tf_op jit(solution)/shard_map/layer/pallas_call | solution.py:468
  73.1 1.8 %copy.9 = bf16[64,3072]{1,0:T(8,128)(2,1)} copy(bf16[64,3072]{1,0:T(8,128)(2,1)} %get-tuple-element.4) | data formatting | bytes 786432
  74.9 1.3 %copy.10 = f32[2,512]{1,0:T(2,128)} copy(f32[2,512]{1,0:T(2,128)} %get-tuple-element.5) | data formatting | bytes 8192

commit v4 on v3

--- a/solution.py
+++ b/solution.py
@@ -21,7 +21,9 @@
 X_ORDER = [0] + [v for s in range(1, NZ // 2) for v in (s, NZ - s)] + [NZ // 2]
 
 
-Q_LAG = 4
+Y_LAG = 2
+Y_DONE = 4
+Z_FLOWS = (2, 1, 0)
 DIRECT = (NZ // 2 - 1, NZ // 2, NZ // 2 + 1)
 
 
@@ -36,8 +38,8 @@
 
 
 def layer_kernel(
-    tokens, wq, wk_in, wv, wo, mixed, lse_out,
-    tok, wz, wog, wox, halo, qf, kvf, oa, ma, la, att, lse_rows, att_b, att_x, part, part_b, part_x,
+    tokens, wq, wk_in, wv, wo, ours, theirs, lse_out,
+    tok, wz, wog, wox, halo, qf, kvf, oa, ma, la, att, lse_rows, att_b, att_x, part, part_b,
     bias_a, bias_b,
     load_sem, out_sem, row_r, zr, yr, yd, push_r, o_r, xr, xd, hr, ar, cr,
 ):
@@ -45,19 +47,19 @@
     sp = z * NY + y
     shard, lanes = wk_in.shape
     rows = tokens.shape[0]
-    other = pl.ds(0, 2 * lanes)
-    mine = pl.ds(2 * lanes, 2 * lanes)
+    other = pl.ds(0, 3 * lanes)
+    mine = pl.ds(3 * lanes, 3 * lanes)
 
     def load(src, dst, k):
         return pltpu.make_async_copy(src, dst, load_sem.at[k])
 
     def loads(first):
-        lo, slot = (0, 1) if first else (2 * lanes, 0)
+        lo, slot = (0, 1) if first else (3 * lanes, 0)
         return [
             load(wk_in, wz.at[sp, :, pl.ds(lo, lanes)], 1),
             load(wv, wz.at[sp, :, pl.ds(lo + lanes, lanes)], 2),
-            load(wo, wog.at[slot, sp], 3),
-            load(wq, wog.at[slot + 2, sp], 4),
+            load(wq, wz.at[sp, :, pl.ds(lo + 2 * lanes, lanes)], 3),
+            load(wo, wog.at[slot, sp], 4),
         ]
 
     for core in (0, 1):
@@ -117,15 +119,15 @@
         remote(ref, ref, sem, xd, z_to[0]).wait_send()
 
     def z_ref(flow, src, way, s):
-        if flow < 2:
+        if flow < 3:
             lo, n = (2 * flow, 2) if s < last else (2 * flow + way, 1)
             return wz.at[src * NY + y, :, pl.ds(lo * lanes, n * lanes)]
         cols = pl.ds(src * NY, NY) if s < last else pl.ds(src * NY + 2 * way, 2)
-        return wog.at[flow - 2, cols]
+        return wog.at[flow - 3, cols]
 
     def z_copy(flow, way, s, hop):
         ref = z_ref(flow, at_z(-hop if way == 0 else hop), way, s)
-        return remote(ref, ref, out_sem.at[flow // 2], zr.at[flow, way, s - 1], z_to[way])
+        return remote(ref, ref, out_sem.at[flow // 3], zr.at[flow, way, s - 1], z_to[way])
 
     def z_first(flow):
         for way in (0, 1):
@@ -139,13 +141,15 @@
 
     def y_copy(kind, slot, col):
         ref = wz.at[at_z(-slot) * NY + at_y(col)]
-        split = 2 * lanes
+        split = 3 * lanes
         if kind == 2:
             ref = ref.at[:, pl.ds(0, split)]
         if kind == 3:
-            ref = ref.at[:, pl.ds(split, 2 * lanes)]
+            ref = ref.at[:, pl.ds(split, 3 * lanes)]
         to = {"y": at_y(2)} if kind == 4 else y_to[kind % 2]
-        return remote(ref, ref, out_sem.at[3], yr.at[kind, slot] if kind < 2 else yd.at[slot], to)
+        return remote(
+            ref, ref, out_sem.at[3 if kind < 2 else 2], yr.at[kind, slot] if kind < 2 else yd.at[slot], to
+        )
 
     def y_send(slot):
         y_copy(0, slot, 0).start()
@@ -170,16 +174,6 @@
         row = pl.ds(at_z(-slot) * NY, NY)
         group = X_ORDER.index(slot) // 4
         remote(wog.at[1, row], wog.at[0, row], out_sem.at[5], o_r.at[group], partner).start()
-
-    def q_push(slot):
-        row = pl.ds(at_z(-slot) * NY, NY)
-        remote(wog.at[3, row], wog.at[2, row], out_sem.at[6], push_r.at[1], partner).start()
-
-    def q_hop(s):
-        for flow in (4, 5):
-            z_hop(flow, s)
-        for slot in arrived(s):
-            q_push(slot)
 
     def arrived(s):
         if s == 0:
@@ -212,9 +206,8 @@
 
     @pl.when(c == 0)
     def _():
+        remote(wz.at[sp, :, other], wz.at[sp, :, other], out_sem.at[0], push_r.at[0], partner).start()
         remote(wog.at[1, sp], wog.at[1, sp], out_sem.at[1], push_r.at[1], partner).start()
-        remote(wz.at[sp, :, other], wz.at[sp, :, other], out_sem.at[0], push_r.at[0], partner).start()
-        remote(wog.at[3, sp], wog.at[3, sp], out_sem.at[2], push_r.at[2], partner).start()
         for group in range(4):
             arrived_all(wog.at[0, pl.ds(0, 4 * NY)], o_r.at[group])
             for slot in X_ORDER[4 * group:4 * group + 4]:
@@ -223,55 +216,51 @@
 
     @pl.when(c == 1)
     def _():
-        z_first(1)
+        z_first(2)
         for d in (1, 3, 2):
             row_send(0, d).start()
+        arrived_all(wz.at[sp, :, other], push_r.at[0])
+        z_first(0)
+        z_first(1)
+        y_send(0)
         arrived_all(wog.at[1, sp], push_r.at[1])
         for d in (1, 3, 2):
             row_send(1, d).start()
-        arrived_all(wz.at[sp, :, other], push_r.at[0])
-        z_first(0)
-        y_send(0)
-        arrived_all(wog.at[3, sp], push_r.at[2])
-        for item in (2, 3):
-            for d in (1, 3, 2):
-                row_send(item, d).start()
         for s in range(1, last + 2):
             if s <= last:
-                for flow in (1, 0):
+                for flow in Z_FLOWS:
                     z_hop(flow, s)
                 for slot in arrived(s):
                     y_send(slot)
             for item in (0, 1):
                 if s == 1:
                     arrived_all(wog.at[0, pl.ds(0, NY - 1)], row_r.at[item])
-                    z_first(2 + item)
+                    z_first(3 + item)
                 else:
-                    z_hop(2 + item, s - 1)
+                    z_hop(3 + item, s - 1)
             for slot in arrived(s - 1):
                 x_send(slot)
                 o_push(slot)
-            if s == Q_LAG:
-                for item in (2, 3):
-                    arrived_all(wog.at[0, pl.ds(0, NY - 1)], row_r.at[item])
-                    z_first(2 + item)
-                q_push(0)
-            if s > Q_LAG:
-                q_hop(s - Q_LAG)
-            for slot in arrived(s - 1):
-                y_relay(slot)
-            if s > 1:
-                for slot in arrived(s - 2):
+            if s >= Y_LAG:
+                for slot in arrived(s - Y_LAG):
+                    y_relay(slot)
+            if s >= Y_DONE:
+                for slot in arrived(s - Y_DONE):
                     y_done(slot)
-        for slot in arrived(last):
-            y_done(slot)
-
+        for s in range(last + 2, last + Y_DONE + 1):
+            if s <= last + Y_LAG:
+                for slot in arrived(s - Y_LAG):
+                    y_relay(slot)
+            for slot in arrived(s - Y_DONE):
+                y_done(slot)
+
+    x_relay(0)
     copy_tokens.wait()
     depth = NZ * NY * shard
-    kv = jnp.dot(tok[...], wz[:, :, 2 * lanes:].reshape(depth, 2 * lanes), preferred_element_type=F32)
+    qkv = jnp.dot(tok[...], wz[:, :, 3 * lanes:].reshape(depth, 3 * lanes), preferred_element_type=F32)
     for j in range(2):
         side = slice(j * lanes, (j + 1) * lanes)
-        kvf[j, WINDOW:, :] = kv[:, side]
+        kvf[j, WINDOW:, :] = qkv[:, side]
         for e in range(4):
             for b in range(4):
                 picked = kvf[j, pl.ds(WINDOW + 4 * b + e, 32, stride=16), :]
@@ -285,11 +274,6 @@
 
     def relay_copy(e, k):
         return remote(halo.at[e, k], halo.at[e, 2], out_sem.at[12], hr.at[2, e], y_to[0 if k == 1 else 1])
-
-    def q_next(s):
-        @pl.when(c == 1)
-        def _():
-            q_hop(s)
 
     for e in range(4):
         prev_copy(e).start()
@@ -318,27 +302,12 @@
         def _():
             relay_copy(e, 3).start()
 
-    done = last + 1 - Q_LAG
-    q_next(done + 1)
-    wrap(0)
-    wrap(1)
-    for s in range(done + 2, last):
-        q_next(s)
-    wrap(2)
-    wrap(3)
-    q_next(last)
-    x_relay(0)
-    pass_on(0)
-    pass_on(1)
-
-    @pl.when(c == 0)
-    def _():
-        arrived_all(wog.at[2], push_r.at[1])
-
-    q = jnp.dot(tok[...], wog[2].reshape(depth, lanes), preferred_element_type=F32)
-    qf[...] = q.astype(BF16).astype(F32) * (HEAD ** -0.5)
-    pass_on(2)
-    pass_on(3)
+    qf[...] = qkv[:, 2 * lanes:].astype(BF16).astype(F32) * (HEAD ** -0.5)
+    for e in range(4):
+        wrap(e)
+    x_relay(1)
+    for e in range(4):
+        pass_on(e)
 
     head0 = lax.broadcasted_iota(jnp.int32, (WINDOW, lanes), 1) < HEAD
 
@@ -373,7 +342,6 @@
         ma[span, :] = top
         la[span, :] = total
 
-    x_relay(1)
 
     for e in range(4):
         row_copy(e, 2, 0).wait_recv()
@@ -405,44 +373,41 @@
     lse_t = lse_rows[...].T
     lse_out[0:1, :] = lse_t[0:1, :]
     lse_out[1:2, :] = lse_t[HEAD:HEAD + 1, :]
-    arrived_all(wox.at[1], xd)
-    arrived_all(att_x.at[pl.ds(1, NX - 1)], ar)
-
     groups = 8
     width = NZ * NY // groups
     hrows = rows // NX // 2
+    for g in range(groups):
+        w_own = wog[0, g * width:(g + 1) * width].reshape(width * shard, lanes)
+        part[g] = nt_dot(att_x[0], w_own).reshape(2, hrows, width * shard)
+    arrived_all(wox.at[1], xd)
+    arrived_all(att_x.at[pl.ds(1, NX - 1)], ar)
 
     def core_copy(j):
-        return remote(part_b.at[j, 1 - c], part_x.at[j], out_sem.at[11], cr.at[j], {"c": 1 - c})
+        return remote(part_b.at[j, 1 - c], theirs.at[j], out_sem.at[11], cr, {"c": 1 - c})
 
     for g in range(groups):
         span = slice(g * width, (g + 1) * width)
-        acc = nt_dot(att_x[0], wog[0, span].reshape(width * shard, lanes))
-        for k in range(1, NX):
+        acc = nt_dot(att_x[1], wox[0, span].reshape(width * shard, lanes))
+        for k in range(2, NX):
             acc += nt_dot(att_x[k], wox[k - 1, span].reshape(width * shard, lanes))
-        acc = acc.reshape(2, hrows, width * shard)
-        part[g] = acc
-        part_b[g] = acc.astype(BF16)
+        part_b[g] = (acc.reshape(2, hrows, width * shard) + part[g]).astype(BF16)
         core_copy(g).start()
-    for g in range(groups):
-        core_copy(g).wait_recv()
-        mixed[:, g * width * shard:(g + 1) * width * shard] = (part[g, c] + part_x[g].astype(F32)).astype(BF16)
-
+    pltpu.make_async_copy(part_b.at[:, c], ours, load_sem.at[1]).start()
+    remote(part_b.at[:, c], theirs, out_sem.at[11], cr, partner).wait_recv()
+    pltpu.make_async_copy(part_b.at[:, c], ours, load_sem.at[1]).wait()
     @pl.when(c == 0)
     def _():
         left_all(wz.at[sp, :, other], out_sem.at[0])
         left_all(wog.at[1, sp], out_sem.at[1])
-        left_all(wog.at[3, sp], out_sem.at[2])
 
     @pl.when(c == 1)
     def _():
         left_all(wz.at[pl.ds(0, NZ - 1)], out_sem.at[0])
-        for k in (1, 2):
-            left_all(wog.at[pl.ds(0, 2), pl.ds(0, (NZ - 1) * NY)], out_sem.at[k])
-        left_all(wz.at[pl.ds(0, 3 * NZ)], out_sem.at[3])
+        left_all(wog.at[:, pl.ds(0, (NZ - 1) * NY)], out_sem.at[1])
+        left_all(wz.at[pl.ds(0, 2 * NZ)], out_sem.at[3])
+        left_all(wz.at[pl.ds(0, NZ)], out_sem.at[2])
         left_all(wz.at[:, :, mine], out_sem.at[4])
-        for k in (5, 6):
-            left_all(wog.at[0], out_sem.at[k])
+        left_all(wog.at[0], out_sem.at[5])
         left_all(wog.at[:, pl.ds(0, NY - 1)], out_sem.at[8])
 
     left_all(wox, out_sem.at[7])
@@ -454,7 +419,15 @@
         left_all(halo.at[:, 0], out_sem.at[12])
 
     left_all(att_x.at[pl.ds(1, NX - 1)], out_sem.at[10])
-    left_all(part_x, out_sem.at[11])
+    left_all(part_b.at[:, c], out_sem.at[11])
+
+
+def sum_kernel(ours, theirs, lse, mixed, lse_out):
+    wide = ours.shape[2]
+    for g in range(ours.shape[0]):
+        total = ours[g].astype(F32) + theirs[g].astype(F32)
+        mixed[:, g * wide:(g + 1) * wide] = total.astype(BF16)
+    lse_out[...] = lse[...]
 
 
 def shards(tokens, w_query, w_key, w_value, w_out):
@@ -464,20 +437,22 @@
     groups = 8
     wide = n_sp // groups * shard
     vmem = pl.BlockSpec(memory_space=pltpu.VMEM)
+    anywhere = pl.BlockSpec(memory_space=pl.ANY)
     dma = pltpu.SemaphoreType.DMA
-    return pl.pallas_call(
+    ours, theirs, lse = pl.pallas_call(
         layer_kernel,
         name="layer",
         out_shape=(
-            jax.ShapeDtypeStruct((rows // 8, depth), BF16),
+            jax.ShapeDtypeStruct((groups, rows // 8, wide), BF16),
+            jax.ShapeDtypeStruct((groups, rows // 8, wide), BF16),
             jax.ShapeDtypeStruct((2, rows), F32),
         ),
         in_specs=[pl.BlockSpec(memory_space=pl.ANY)] * 5,
-        out_specs=(vmem, vmem),
+        out_specs=(anywhere, anywhere, vmem),
         scratch_shapes=[
             pltpu.VMEM((rows, depth), BF16),
-            pltpu.VMEM((n_sp, shard, 4 * lanes), BF16),
-            pltpu.VMEM((4, n_sp, shard, lanes), BF16),
+            pltpu.VMEM((n_sp, shard, 6 * lanes), BF16),
+            pltpu.VMEM((2, n_sp, shard, lanes), BF16),
             pltpu.VMEM((NX - 1, n_sp, shard, lanes), BF16),
             pltpu.VMEM((4, 5, WINDOW, 2 * lanes), BF16),
             pltpu.VMEM((rows, lanes), F32),
@@ -491,27 +466,36 @@
             pltpu.VMEM((NX, rows // NX, lanes), BF16),
             pltpu.VMEM((groups, 2, rows // NX // 2, wide), F32),
             pltpu.VMEM((groups, 2, rows // NX // 2, wide), BF16),
-            pltpu.VMEM((groups, rows // NX // 2, wide), BF16),
             pltpu.VMEM((2, WINDOW, 2 * WINDOW), F32),
             pltpu.VMEM((WINDOW, 5 * WINDOW), F32),
             dma((5,)),
             dma((13,)),
-            dma((4,)),
-            dma((6, 2, NZ // 2)),
+            dma((2,)),
+            dma((5, 2, NZ // 2)),
             dma((2, NZ)),
             dma((NZ,)),
-            dma((3,)),
+            dma((2,)),
             dma((4,)),
             dma((2, 2)),
             dma,
             dma((4, 4)),
             dma,
-            dma((groups,)),
+            dma,
         ],
         compiler_params=pltpu.CompilerParams(
             collective_id=0, has_side_effects=True, vmem_limit_bytes=60 * 1024 * 1024
         ),
     )(tokens, w_query, w_key, w_value, w_out.T)
+    return pl.pallas_call(
+        sum_kernel,
+        name="total",
+        out_shape=(
+            jax.ShapeDtypeStruct((rows // 8, depth), BF16),
+            jax.ShapeDtypeStruct((2, rows), F32),
+        ),
+        in_specs=[vmem] * 3,
+        out_specs=(vmem, vmem),
+    )(ours, theirs, lse)
 
 
 def solution(mesh):

time: 76.4 us -> 73.4 us (0.961)
  local copies, waits for them, and re-layouts: 3.03 us -> 0 us
    unnamed x2 -> x0, local copies, waits for them, and re-layouts: 3.03 us -> none
    pallas_call x0 -> x1, Pallas kernels: none -> 1.96 us  [shards(): pl.pallas_call(sum_kernel, name='total', out_shape=(jax.ShapeDtypeStruct(...]
    pallas_call x1, Pallas kernels: 72.5 us -> 70.6 us  [shards(): pl.pallas_call(layer_kernel, name='layer', out_shape=(jax.ShapeDtypeStruc...]
where the time goes in v4:
time: 73.4 us; the launch traced here: 73.2 us
  Pallas kernels  72.6 us (99%)
    pallas_call x1, Pallas kernels, shards(): pl.pallas_call(layer_kernel, name='layer', out_shape=(jax.ShapeDtypeStruc...  70.6 us
    pallas_call x1, Pallas kernels, shards(): pl.pallas_call(sum_kernel, name='total', out_shape=(jax.ShapeDtypeStruct(...  1.96 us

profile of v4, /device:TPU:1, one launch (start us, length us, event | category | flops | bytes accessed | tf_op | source)
XLA Modules:
  0.0 73.2 jit_solution(5876756901865646192)
XLA Ops:
  0.6 70.6 %layer.1 = (bf16[8,64,384]{2,1,0:T(8,128)(2,1)}, bf16[8,64,384]{2,1,0:T(8,128)(2,1)}, f32[2,512]{1,0:T(2,128)}) custom-call(bf16[512,3072]{1,0:T(8,128)(2,1)} %tokens.1, bf16[48,128]{1,0:T(8,128)(2,1)} %wq.1, bf16[48,128]{1,0:T(8,128)(2,1)} %wk_in.1, bf16[48,128]{1,0:T(8,128)(2,1)} %wv.1, bf16[48,128]{1,0:T(8,128)(2,1)} %bitcast.1), custom_call_target="tpu_custom_call" | custom-call | tf_op jit(solution)/shard_map/layer/pallas_call | solution.py:442
  71.2 2.0 %total.1 = (bf16[64,3072]{1,0:T(8,128)(2,1)}, f32[2,512]{1,0:T(2,128)}) custom-call(bf16[8,64,384]{2,1,0:T(8,128)(2,1)} %get-tuple-element.5.ours, bf16[8,64,384]{2,1,0:T(8,128)(2,1)} %get-tuple-element.6.theirs, f32[2,512]{1,0:T(2,128)} %get-tuple-element.7.lse), custom_call_target="tpu_custom_call" | custom-call | tf_op jit(solution)/shard_map/total/pallas_call | solution.py:489

commit v5 on v4

--- a/solution.py
+++ b/solution.py
@@ -21,10 +21,11 @@
 X_ORDER = [0] + [v for s in range(1, NZ // 2) for v in (s, NZ - s)] + [NZ // 2]
 
 
-Y_LAG = 2
-Y_DONE = 4
+O_LAG = 1
+Y_LAG = 1
+Y_DONE = 3
 Z_FLOWS = (2, 1, 0)
-DIRECT = (NZ // 2 - 1, NZ // 2, NZ // 2 + 1)
+DIRECT = (NZ // 2,)
 
 
 def nt_dot(a, b):
@@ -39,7 +40,7 @@
 
 def layer_kernel(
     tokens, wq, wk_in, wv, wo, ours, theirs, lse_out,
-    tok, wz, wog, wox, halo, qf, kvf, oa, ma, la, att, lse_rows, att_b, att_x, part, part_b,
+    tok, acc, wz, wog, wox, halo, qf, kvf, oa, ma, la, att, lse_rows, att_b, att_x, part, part_b,
     bias_a, bias_b,
     load_sem, out_sem, row_r, zr, yr, yd, push_r, o_r, xr, xd, hr, ar, cr,
 ):
@@ -168,7 +169,9 @@
     def y_done(slot):
         y_copy(4, slot, 2).wait_recv()
         row = pl.ds(at_z(-slot) * NY, NY)
-        remote(wz.at[row, :, other], wz.at[row, :, mine], out_sem.at[4], push_r.at[0], partner).start()
+        near = min(slot, NZ - slot)
+        group = 0 if near <= 4 else 1 if near <= 6 else 2
+        remote(wz.at[row, :, other], wz.at[row, :, mine], out_sem.at[4], push_r.at[group], partner).start()
 
     def o_push(slot):
         row = pl.ds(at_z(-slot) * NY, NY)
@@ -204,19 +207,34 @@
         ref = wog.at[item, sp]
         return remote(ref, ref, out_sem.at[8], row_r.at[item], {"y": at_y(d)})
 
+    first = z - 4 + lax.rem(z, 2)
+
+    def project(k):
+        src = lax.rem(first + 2 * k + NZ, NZ)
+        at = pl.multiple_of(src * (NY * shard), 2 * NY * shard)
+        w = wz[pl.ds(src * NY, 2 * NY), :, 3 * lanes:].reshape(2 * NY * shard, 3 * lanes)
+        return jnp.dot(tok[:, pl.ds(at, 2 * NY * shard)], w, preferred_element_type=F32)
+
     @pl.when(c == 0)
     def _():
         remote(wz.at[sp, :, other], wz.at[sp, :, other], out_sem.at[0], push_r.at[0], partner).start()
         remote(wog.at[1, sp], wog.at[1, sp], out_sem.at[1], push_r.at[1], partner).start()
+        copy_tokens.wait()
         for group in range(4):
             arrived_all(wog.at[0, pl.ds(0, 4 * NY)], o_r.at[group])
             for slot in X_ORDER[4 * group:4 * group + 4]:
                 x_send(slot)
-        arrived_all(wz.at[:, :, mine], push_r.at[0])
+            if group == 2:
+                arrived_all(wz.at[pl.ds(0, 9 * NY), :, mine], push_r.at[0])
+                acc[...] = project(0) + project(1) + project(2) + project(3)
+        arrived_all(wz.at[pl.ds(0, 4 * NY), :, mine], push_r.at[1])
+        acc[...] += project(-1) + project(4)
+        arrived_all(wz.at[pl.ds(0, 3 * NY), :, mine], push_r.at[2])
 
     @pl.when(c == 1)
     def _():
         z_first(2)
+        copy_tokens.wait()
         for d in (1, 3, 2):
             row_send(0, d).start()
         arrived_all(wz.at[sp, :, other], push_r.at[0])
@@ -226,7 +244,7 @@
         arrived_all(wog.at[1, sp], push_r.at[1])
         for d in (1, 3, 2):
             row_send(1, d).start()
-        for s in range(1, last + 2):
+        for s in range(1, last + O_LAG + 1):
             if s <= last:
                 for flow in Z_FLOWS:
                     z_hop(flow, s)
@@ -236,18 +254,22 @@
                 if s == 1:
                     arrived_all(wog.at[0, pl.ds(0, NY - 1)], row_r.at[item])
                     z_first(3 + item)
-                else:
-                    z_hop(3 + item, s - 1)
-            for slot in arrived(s - 1):
+                elif s > O_LAG:
+                    z_hop(3 + item, s - O_LAG)
+            for slot in [0] if s == 1 else arrived(s - O_LAG) if s > O_LAG else []:
                 x_send(slot)
                 o_push(slot)
-            if s >= Y_LAG:
+            if Y_LAG <= s <= last + Y_LAG:
                 for slot in arrived(s - Y_LAG):
                     y_relay(slot)
-            if s >= Y_DONE:
+            if Y_DONE <= s <= last + Y_DONE:
                 for slot in arrived(s - Y_DONE):
                     y_done(slot)
-        for s in range(last + 2, last + Y_DONE + 1):
+            if s == 4 + Y_DONE:
+                acc[...] = project(0) + project(1) + project(2) + project(3)
+            if s == 6 + Y_DONE:
+                acc[...] += project(-1) + project(4)
+        for s in range(last + O_LAG + 1, last + Y_DONE + 1):
             if s <= last + Y_LAG:
                 for slot in arrived(s - Y_LAG):
                     y_relay(slot)
@@ -255,9 +277,7 @@
                 y_done(slot)
 
     x_relay(0)
-    copy_tokens.wait()
-    depth = NZ * NY * shard
-    qkv = jnp.dot(tok[...], wz[:, :, 3 * lanes:].reshape(depth, 3 * lanes), preferred_element_type=F32)
+    qkv = acc[...] + project(5) + project(6)
     for j in range(2):
         side = slice(j * lanes, (j + 1) * lanes)
         kvf[j, WINDOW:, :] = qkv[:, side]
@@ -278,7 +298,7 @@
     for e in range(4):
         prev_copy(e).start()
         for k in (1, 3):
-            @pl.when(y + k < NY)
+            @pl.when((y + k < NY) & ((c == 0) | (e < 2)))
             def _():
                 row_copy(e, k, 0).start()
 
@@ -303,12 +323,6 @@
             relay_copy(e, 3).start()
 
     qf[...] = qkv[:, 2 * lanes:].astype(BF16).astype(F32) * (HEAD ** -0.5)
-    for e in range(4):
-        wrap(e)
-    x_relay(1)
-    for e in range(4):
-        pass_on(e)
-
     head0 = lax.broadcasted_iota(jnp.int32, (WINDOW, lanes), 1) < HEAD
 
     def attend(qb, kb, vb, bias):
@@ -327,12 +341,7 @@
         out = jnp.where(head0, o[0:WINDOW], o[WINDOW:])
         return out, jnp.where(head0, tops[0], tops[1]), jnp.where(head0, sums[0], sums[1])
 
-    for e in range(4):
-        for b in range(4):
-            for j in range(2):
-                tail = halo[e, 1, 32 * b + 24:32 * b + 32, j * lanes:(j + 1) * lanes]
-                kvf[j, pl.ds(4 * b + e, 8, stride=16), :] = tail.astype(F32)
-    for i in range(rows // WINDOW):
+    def near_block(i):
         span = slice(i * WINDOW, (i + 1) * WINDOW)
         keys = slice(i * WINDOW, (i + 2) * WINDOW)
         out, top, total = attend(
@@ -342,6 +351,25 @@
         ma[span, :] = top
         la[span, :] = total
 
+    for e in range(4):
+        wrap(e)
+        if e < 2:
+            for k in (1, 3):
+                @pl.when((y + k < NY) & (c == 1))
+                def _():
+                    row_copy(e + 2, k, 0).start()
+        if e < 3:
+            near_block(e + 1)
+    x_relay(1)
+    for e in range(4):
+        pass_on(e)
+
+    for e in range(4):
+        for b in range(4):
+            for j in range(2):
+                tail = halo[e, 1, 32 * b + 24:32 * b + 32, j * lanes:(j + 1) * lanes]
+                kvf[j, pl.ds(4 * b + e, 8, stride=16), :] = tail.astype(F32)
+    near_block(0)
 
     for e in range(4):
         row_copy(e, 2, 0).wait_recv()
@@ -365,7 +393,7 @@
     att_b[...] = att[...].reshape(NX, rows // NX, lanes).astype(BF16)
 
     def att_copy(d):
-        return remote(att_b.at[at_x(d)], att_x.at[NX - d], out_sem.at[10], ar, {"x": at_x(d)})
+        return remote(att_b.at[at_x(d)], att_x.at[NX - d], out_sem.at[10], ar.at[d - 1], {"x": at_x(d)})
 
     for d in (1, 3, 2):
         att_copy(d).start()
@@ -379,19 +407,24 @@
     for g in range(groups):
         w_own = wog[0, g * width:(g + 1) * width].reshape(width * shard, lanes)
         part[g] = nt_dot(att_x[0], w_own).reshape(2, hrows, width * shard)
+    for d in (1, 3):
+        att_copy(NX - d).wait_recv()
+        for g in range(groups):
+            w_k = wox[d - 1, g * width:(g + 1) * width].reshape(width * shard, lanes)
+            part[g] += nt_dot(att_x[d], w_k).reshape(2, hrows, width * shard)
     arrived_all(wox.at[1], xd)
-    arrived_all(att_x.at[pl.ds(1, NX - 1)], ar)
+    att_copy(2).wait_recv()
 
     def core_copy(j):
-        return remote(part_b.at[j, 1 - c], theirs.at[j], out_sem.at[11], cr, {"c": 1 - c})
+        at = pl.ds(j * groups // 2, groups // 2)
+        return remote(part_b.at[at, 1 - c], theirs.at[at], out_sem.at[11], cr, {"c": 1 - c})
 
     for g in range(groups):
         span = slice(g * width, (g + 1) * width)
-        acc = nt_dot(att_x[1], wox[0, span].reshape(width * shard, lanes))
-        for k in range(2, NX):
-            acc += nt_dot(att_x[k], wox[k - 1, span].reshape(width * shard, lanes))
+        acc = nt_dot(att_x[2], wox[1, span].reshape(width * shard, lanes))
         part_b[g] = (acc.reshape(2, hrows, width * shard) + part[g]).astype(BF16)
-        core_copy(g).start()
+        if g % (groups // 2) == groups // 2 - 1:
+            core_copy(g * 2 // groups).start()
     pltpu.make_async_copy(part_b.at[:, c], ours, load_sem.at[1]).start()
     remote(part_b.at[:, c], theirs, out_sem.at[11], cr, partner).wait_recv()
     pltpu.make_async_copy(part_b.at[:, c], ours, load_sem.at[1]).wait()
@@ -451,6 +484,7 @@
         out_specs=(anywhere, anywhere, vmem),
         scratch_shapes=[
             pltpu.VMEM((rows, depth), BF16),
+            pltpu.VMEM((rows, 3 * lanes), F32),
             pltpu.VMEM((n_sp, shard, 6 * lanes), BF16),
             pltpu.VMEM((2, n_sp, shard, lanes), BF16),
             pltpu.VMEM((NX - 1, n_sp, shard, lanes), BF16),
@@ -474,12 +508,12 @@
             dma((5, 2, NZ // 2)),
             dma((2, NZ)),
             dma((NZ,)),
-            dma((2,)),
+            dma((3,)),
             dma((4,)),
             dma((2, 2)),
             dma,
             dma((4, 4)),
-            dma,
+            dma((3,)),
             dma,
         ],
         compiler_params=pltpu.CompilerParams(

time: 73.4 us -> 70.5 us (0.960)
  Pallas kernels: 72.6 us -> 69.6 us
    pallas_call x1, Pallas kernels: 70.6 us -> 67.7 us  [shards(): pl.pallas_call(layer_kernel, name='layer', out_shape=(jax.ShapeDtypeStruc...]
where the time goes in v5:
time: 70.5 us; the launch traced here: 70.3 us
  Pallas kernels  69.6 us (99%)
    pallas_call x1, Pallas kernels, shards(): pl.pallas_call(layer_kernel, name='layer', out_shape=(jax.ShapeDtypeStruc...  67.7 us
    pallas_call x1, Pallas kernels, shards(): pl.pallas_call(sum_kernel, name='total', out_shape=(jax.ShapeDtypeStruct(...  1.96 us

profile of v5, /device:TPU:1, one launch (start us, length us, event | category | flops | bytes accessed | tf_op | source)
XLA Modules:
  0.0 70.3 jit_solution(18228419036565276488)
XLA Ops:
  0.6 67.7 %layer.1 = (bf16[8,64,384]{2,1,0:T(8,128)(2,1)}, bf16[8,64,384]{2,1,0:T(8,128)(2,1)}, f32[2,512]{1,0:T(2,128)}) custom-call(bf16[512,3072]{1,0:T(8,128)(2,1)} %tokens.1, bf16[48,128]{1,0:T(8,128)(2,1)} %wq.1, bf16[48,128]{1,0:T(8,128)(2,1)} %wk_in.1, bf16[48,128]{1,0:T(8,128)(2,1)} %wv.1, bf16[48,128]{1,0:T(8,128)(2,1)} %bitcast.1), custom_call_target="tpu_custom_call" | custom-call | tf_op jit(solution)/shard_map/layer/pallas_call | solution.py:475
  68.3 2.0 %total.1 = (bf16[64,3072]{1,0:T(8,128)(2,1)}, f32[2,512]{1,0:T(2,128)}) custom-call(bf16[8,64,384]{2,1,0:T(8,128)(2,1)} %get-tuple-element.5.ours, bf16[8,64,384]{2,1,0:T(8,128)(2,1)} %get-tuple-element.6.theirs, f32[2,512]{1,0:T(2,128)} %get-tuple-element.7.lse), custom_call_target="tpu_custom_call" | custom-call | tf_op jit(solution)/shard_map/total/pallas_call | solution.py:523

commit v6 on v5

--- a/solution.py
+++ b/solution.py
@@ -40,7 +40,7 @@
 
 def layer_kernel(
     tokens, wq, wk_in, wv, wo, ours, theirs, lse_out,
-    tok, acc, wz, wog, wox, halo, qf, kvf, oa, ma, la, att, lse_rows, att_b, att_x, part, part_b,
+    tok, acc, wz, wog, wox, halo, qf, kvf, oa, ma, la, att, lse_rows, lse_v, att_b, att_x, part, part_b,
     bias_a, bias_b,
     load_sem, out_sem, row_r, zr, yr, yd, push_r, o_r, xr, xd, hr, ar, cr,
 ):
@@ -85,6 +85,7 @@
     peers += [{"y": at_y(d)} for d in range(1, NY)]
     peers += [{"x": at_x(d)} for d in range(1, NX)]
     peers += [{"c": 1 - c}]
+    peers += [{"z": at_z(d), "c": 1 - c} for d in (1, -1)] + [{"y": at_y(d), "c": 1 - c} for d in range(1, NY)]
     for peer in peers:
         pl.semaphore_signal(barrier, inc=1, device_id=peer, device_id_type=MESH)
     r = lax.broadcasted_iota(jnp.int32, (WINDOW, 2 * WINDOW), 0)
@@ -215,10 +216,20 @@
         w = wz[pl.ds(src * NY, 2 * NY), :, 3 * lanes:].reshape(2 * NY * shard, 3 * lanes)
         return jnp.dot(tok[:, pl.ds(at, 2 * NY * shard)], w, preferred_element_type=F32)
 
+    def first_sends(ref):
+        for way in (0, 1):
+            remote(ref, ref, out_sem.at[0], zr.at[0, way, 0], {"z": at_z(1 - 2 * way), "c": 1}).start()
+        for kind in (0, 1):
+            remote(ref, ref, out_sem.at[0], yr.at[kind, 0], {"y": at_y(1 - 2 * kind), "c": 1}).start()
+
     @pl.when(c == 0)
     def _():
+        first_sends(wz.at[sp, :, other])
+        for d in (1, 3, 2):
+            at = {"y": at_y(d), "c": 1}
+            remote(wog.at[1, sp], wog.at[1, sp], out_sem.at[1], row_r.at[1], at).start()
+        remote(wog.at[1, sp], wog.at[1, sp], out_sem.at[1], push_r.at[1], partner).start()
         remote(wz.at[sp, :, other], wz.at[sp, :, other], out_sem.at[0], push_r.at[0], partner).start()
-        remote(wog.at[1, sp], wog.at[1, sp], out_sem.at[1], push_r.at[1], partner).start()
         copy_tokens.wait()
         for group in range(4):
             arrived_all(wog.at[0, pl.ds(0, 4 * NY)], o_r.at[group])
@@ -233,21 +244,22 @@
 
     @pl.when(c == 1)
     def _():
-        z_first(2)
-        copy_tokens.wait()
+        first_sends(wz.at[sp, :, mine])
         for d in (1, 3, 2):
             row_send(0, d).start()
+        copy_tokens.wait()
+        arrived_all(wog.at[1, sp], push_r.at[1])
         arrived_all(wz.at[sp, :, other], push_r.at[0])
-        z_first(0)
-        z_first(1)
-        y_send(0)
-        arrived_all(wog.at[1, sp], push_r.at[1])
-        for d in (1, 3, 2):
-            row_send(1, d).start()
         for s in range(1, last + O_LAG + 1):
             if s <= last:
-                for flow in Z_FLOWS:
-                    z_hop(flow, s)
+                if s == 1:
+                    for way in (0, 1):
+                        arrived_all(wz.at[sp], zr.at[0, way, 0])
+                        for flow in Z_FLOWS:
+                            z_copy(flow, way, 2, 1).start()
+                else:
+                    for flow in Z_FLOWS:
+                        z_hop(flow, s)
                 for slot in arrived(s):
                     y_send(slot)
             for item in (0, 1):
@@ -399,8 +411,10 @@
         att_copy(d).start()
     att_x[0] = att_b[x]
     lse_t = lse_rows[...].T
-    lse_out[0:1, :] = lse_t[0:1, :]
-    lse_out[1:2, :] = lse_t[HEAD:HEAD + 1, :]
+    lse_v[0:1, :] = lse_t[0:1, :]
+    lse_v[1:2, :] = lse_t[HEAD:HEAD + 1, :]
+    copy_lse = pltpu.make_async_copy(lse_v, lse_out, load_sem.at[2])
+    copy_lse.start()
     groups = 8
     width = NZ * NY // groups
     hrows = rows // NX // 2
@@ -428,20 +442,21 @@
     pltpu.make_async_copy(part_b.at[:, c], ours, load_sem.at[1]).start()
     remote(part_b.at[:, c], theirs, out_sem.at[11], cr, partner).wait_recv()
     pltpu.make_async_copy(part_b.at[:, c], ours, load_sem.at[1]).wait()
+    copy_lse.wait()
     @pl.when(c == 0)
     def _():
-        left_all(wz.at[sp, :, other], out_sem.at[0])
-        left_all(wog.at[1, sp], out_sem.at[1])
+        left_all(wz.at[pl.ds(0, 5), :, other], out_sem.at[0])
+        left_all(wog.at[0, pl.ds(0, NY)], out_sem.at[1])
 
     @pl.when(c == 1)
     def _():
         left_all(wz.at[pl.ds(0, NZ - 1)], out_sem.at[0])
         left_all(wog.at[:, pl.ds(0, (NZ - 1) * NY)], out_sem.at[1])
-        left_all(wz.at[pl.ds(0, 2 * NZ)], out_sem.at[3])
+        left_all(wz.at[pl.ds(0, 2 * NZ - 2)], out_sem.at[3])
         left_all(wz.at[pl.ds(0, NZ)], out_sem.at[2])
         left_all(wz.at[:, :, mine], out_sem.at[4])
         left_all(wog.at[0], out_sem.at[5])
-        left_all(wog.at[:, pl.ds(0, NY - 1)], out_sem.at[8])
+        left_all(wog.at[0, pl.ds(0, NY - 1)], out_sem.at[8])
 
     left_all(wox, out_sem.at[7])
     left_all(halo.at[:, pl.ds(0, 3)], out_sem.at[9])
@@ -481,7 +496,7 @@
             jax.ShapeDtypeStruct((2, rows), F32),
         ),
         in_specs=[pl.BlockSpec(memory_space=pl.ANY)] * 5,
-        out_specs=(anywhere, anywhere, vmem),
+        out_specs=(anywhere, anywhere, anywhere),
         scratch_shapes=[
             pltpu.VMEM((rows, depth), BF16),
             pltpu.VMEM((rows, 3 * lanes), F32),
@@ -496,6 +511,7 @@
             pltpu.VMEM((rows, lanes), F32),
             pltpu.VMEM((rows, lanes), F32),
             pltpu.VMEM((rows, lanes), F32),
+            pltpu.VMEM((2, rows), F32),
             pltpu.VMEM((NX, rows // NX, lanes), BF16),
             pltpu.VMEM((NX, rows // NX, lanes), BF16),
             pltpu.VMEM((groups, 2, rows // NX // 2, wide), F32),

time: 70.5 us -> 69.7 us (0.989)
    pallas_call x1, Pallas kernels: 67.7 us -> 66.9 us  [shards(): pl.pallas_call(layer_kernel, name='layer', out_shape=(jax.ShapeDtypeStruc...]
where the time goes in v6:
time: 69.7 us; the launch traced here: 69.5 us
  Pallas kernels  68.9 us (99%)
    pallas_call x1, Pallas kernels, shards(): pl.pallas_call(layer_kernel, name='layer', out_shape=(jax.ShapeDtypeStruc...  66.9 us
    pallas_call x1, Pallas kernels, shards(): pl.pallas_call(sum_kernel, name='total', out_shape=(jax.ShapeDtypeStruct(...  1.96 us

profile of v6, /device:TPU:1, one launch (start us, length us, event | category | flops | bytes accessed | tf_op | source)
XLA Modules:
  0.0 69.5 jit_solution(10111802661052602182)
XLA Ops:
  0.6 66.9 %layer.1 = (bf16[8,64,384]{2,1,0:T(8,128)(2,1)}, bf16[8,64,384]{2,1,0:T(8,128)(2,1)}, f32[2,512]{1,0:T(2,128)}) custom-call(bf16[512,3072]{1,0:T(8,128)(2,1)} %tokens.1, bf16[48,128]{1,0:T(8,128)(2,1)} %wq.1, bf16[48,128]{1,0:T(8,128)(2,1)} %wk_in.1, bf16[48,128]{1,0:T(8,128)(2,1)} %wv.1, bf16[48,128]{1,0:T(8,128)(2,1)} %bitcast.1), custom_call_target="tpu_custom_call" | custom-call | tf_op jit(solution)/shard_map/layer/pallas_call | solution.py:490
  67.6 2.0 %total.1 = (bf16[64,3072]{1,0:T(8,128)(2,1)}, f32[2,512]{1,0:T(2,128)}) custom-call(bf16[8,64,384]{2,1,0:T(8,128)(2,1)} %get-tuple-element.5.ours, bf16[8,64,384]{2,1,0:T(8,128)(2,1)} %get-tuple-element.6.theirs, f32[2,512]{1,0:T(2,128)} %get-tuple-element.7.lse), custom_call_target="tpu_custom_call" | custom-call | tf_op jit(solution)/shard_map/total/pallas_call | solution.py:539

commit v7 on v6

--- a/solution.py
+++ b/solution.py
@@ -40,7 +40,7 @@
 
 def layer_kernel(
     tokens, wq, wk_in, wv, wo, ours, theirs, lse_out,
-    tok, acc, wz, wog, wox, halo, qf, kvf, oa, ma, la, att, lse_rows, lse_v, att_b, att_x, part, part_b,
+    tok, acc, wz, wog, woxs, woxm, halo, qf, kvf, oa, ma, la, att, lse_rows, lse_v, att_b, att_x, part, part_b,
     bias_a, bias_b,
     load_sem, out_sem, row_r, zr, yr, yd, push_r, o_r, xr, xd, hr, ar, cr,
 ):
@@ -187,11 +187,10 @@
     def x_copy(kind, slot):
         span = pl.ds(at_z(-slot) * NY, NY)
         way = (0, 1, slot % 2)[kind]
-        src = wox.at[(2, 0)[way], span] if kind == 2 else wog.at[0, span]
-        dst = wox.at[(2, 0, 1)[kind], span]
+        side = woxs.at[span, :, pl.ds((1 - way) * lanes, lanes)]
         return remote(
-            src, dst, out_sem.at[7], xr.at[kind, X_ORDER.index(slot) // 8] if kind < 2 else xd,
-            {"x": at_x(1 if way == 0 else -1)},
+            side if kind == 2 else wog.at[0, span], woxm.at[span] if kind == 2 else side, out_sem.at[7],
+            xr.at[kind, X_ORDER.index(slot) // 8] if kind < 2 else xd, {"x": at_x(1 if way == 0 else -1)},
         )
 
     def x_send(slot):
@@ -200,7 +199,7 @@
 
     def x_relay(group):
         for kind in (0, 1):
-            arrived_all(wox.at[0, pl.ds(0, 8 * NY)], xr.at[kind, group])
+            arrived_all(woxm.at[pl.ds(0, 8 * NY)], xr.at[kind, group])
         for slot in X_ORDER[8 * group:8 * group + 8]:
             x_copy(2, slot).start()
 
@@ -423,10 +422,11 @@
         part[g] = nt_dot(att_x[0], w_own).reshape(2, hrows, width * shard)
     for d in (1, 3):
         att_copy(NX - d).wait_recv()
-        for g in range(groups):
-            w_k = wox[d - 1, g * width:(g + 1) * width].reshape(width * shard, lanes)
-            part[g] += nt_dot(att_x[d], w_k).reshape(2, hrows, width * shard)
-    arrived_all(wox.at[1], xd)
+    sides = jnp.concatenate([att_x[1], att_x[3]], 1)
+    for g in range(groups):
+        w_k = woxs[g * width:(g + 1) * width].reshape(width * shard, 2 * lanes)
+        part[g] += nt_dot(sides, w_k).reshape(2, hrows, width * shard)
+    arrived_all(woxm, xd)
     att_copy(2).wait_recv()
 
     def core_copy(j):
@@ -435,7 +435,7 @@
 
     for g in range(groups):
         span = slice(g * width, (g + 1) * width)
-        acc = nt_dot(att_x[2], wox[1, span].reshape(width * shard, lanes))
+        acc = nt_dot(att_x[2], woxm[span].reshape(width * shard, lanes))
         part_b[g] = (acc.reshape(2, hrows, width * shard) + part[g]).astype(BF16)
         if g % (groups // 2) == groups // 2 - 1:
             core_copy(g * 2 // groups).start()
@@ -458,7 +458,7 @@
         left_all(wog.at[0], out_sem.at[5])
         left_all(wog.at[0, pl.ds(0, NY - 1)], out_sem.at[8])
 
-    left_all(wox, out_sem.at[7])
+    left_all(wz.at[:, :, mine], out_sem.at[7])
     left_all(halo.at[:, pl.ds(0, 3)], out_sem.at[9])
     left_all(halo.at[0, pl.ds(0, 2)], out_sem.at[12])
 
@@ -502,7 +502,8 @@
             pltpu.VMEM((rows, 3 * lanes), F32),
             pltpu.VMEM((n_sp, shard, 6 * lanes), BF16),
             pltpu.VMEM((2, n_sp, shard, lanes), BF16),
-            pltpu.VMEM((NX - 1, n_sp, shard, lanes), BF16),
+            pltpu.VMEM((n_sp, shard, 2 * lanes), BF16),
+            pltpu.VMEM((n_sp, shard, lanes), BF16),
             pltpu.VMEM((4, 5, WINDOW, 2 * lanes), BF16),
             pltpu.VMEM((rows, lanes), F32),
             pltpu.VMEM((2, WINDOW + rows, lanes), F32),

time: 69.7 us -> 69.6 us (level)
  no operation moved by 1% of the time
where the time goes in v7:
time: 69.6 us; the launch traced here: 69.4 us
  Pallas kernels  68.8 us (99%)
    pallas_call x1, Pallas kernels, shards(): pl.pallas_call(layer_kernel, name='layer', out_shape=(jax.ShapeDtypeStruc...  66.8 us
    pallas_call x1, Pallas kernels, shards(): pl.pallas_call(sum_kernel, name='total', out_shape=(jax.ShapeDtypeStruct(...  1.96 us

profile of v7, /device:TPU:1, one launch (start us, length us, event | category | flops | bytes accessed | tf_op | source)
XLA Modules:
  0.0 69.4 jit_solution(10786797029468858509)
XLA Ops:
  0.6 66.8 %layer.1 = (bf16[8,64,384]{2,1,0:T(8,128)(2,1)}, bf16[8,64,384]{2,1,0:T(8,128)(2,1)}, f32[2,512]{1,0:T(2,128)}) custom-call(bf16[512,3072]{1,0:T(8,128)(2,1)} %tokens.1, bf16[48,128]{1,0:T(8,128)(2,1)} %wq.1, bf16[48,128]{1,0:T(8,128)(2,1)} %wk_in.1, bf16[48,128]{1,0:T(8,128)(2,1)} %wv.1, bf16[48,128]{1,0:T(8,128)(2,1)} %bitcast.1), custom_call_target="tpu_custom_call" | custom-call | tf_op jit(solution)/shard_map/layer/pallas_call | solution.py:490
  67.5 2.0 %total.1 = (bf16[64,3072]{1,0:T(8,128)(2,1)}, f32[2,512]{1,0:T(2,128)}) custom-call(bf16[8,64,384]{2,1,0:T(8,128)(2,1)} %get-tuple-element.5.ours, bf16[8,64,384]{2,1,0:T(8,128)(2,1)} %get-tuple-element.6.theirs, f32[2,512]{1,0:T(2,128)} %get-tuple-element.7.lse), custom_call_target="tpu_custom_call" | custom-call | tf_op jit(solution)/shard_map/total/pallas_call | solution.py:540

commit v8 on v7

--- a/solution.py
+++ b/solution.py
@@ -150,7 +150,8 @@
             ref = ref.at[:, pl.ds(split, 3 * lanes)]
         to = {"y": at_y(2)} if kind == 4 else y_to[kind % 2]
         return remote(
-            ref, ref, out_sem.at[3 if kind < 2 else 2], yr.at[kind, slot] if kind < 2 else yd.at[slot], to
+            ref, ref, out_sem.at[3 if kind < 2 else 2],
+            yr.at[kind, min(slot, NZ - slot)] if kind < 2 else yd.at[min(slot, NZ - slot)], to,
         )
 
     def y_send(slot):
@@ -159,16 +160,19 @@
         if slot in DIRECT:
             y_copy(4, slot, 0).start()
 
-    def y_relay(slot):
-        y_copy(0, slot, -1).wait_recv()
-        if slot not in DIRECT:
-            y_copy(2, slot, -1).start()
-        y_copy(1, slot, 1).wait_recv()
-        if slot not in DIRECT:
-            y_copy(3, slot, 1).start()
-
-    def y_done(slot):
-        y_copy(4, slot, 2).wait_recv()
+    def y_relay(step):
+        for kind, col in ((0, -1), (1, 1)):
+            arrived_all(wz.at[pl.ds(0, len(arrived(step)))], yr.at[kind, step])
+            for slot in arrived(step):
+                if slot not in DIRECT:
+                    y_copy(kind + 2, slot, col).start()
+
+    def y_done(step):
+        arrived_all(wz.at[pl.ds(0, len(arrived(step)))], yd.at[step])
+        for slot in arrived(step):
+            y_push(slot)
+
+    def y_push(slot):
         row = pl.ds(at_z(-slot) * NY, NY)
         near = min(slot, NZ - slot)
         group = 0 if near <= 4 else 1 if near <= 6 else 2
@@ -271,21 +275,17 @@
                 x_send(slot)
                 o_push(slot)
             if Y_LAG <= s <= last + Y_LAG:
-                for slot in arrived(s - Y_LAG):
-                    y_relay(slot)
+                y_relay(s - Y_LAG)
             if Y_DONE <= s <= last + Y_DONE:
-                for slot in arrived(s - Y_DONE):
-                    y_done(slot)
+                y_done(s - Y_DONE)
             if s == 4 + Y_DONE:
                 acc[...] = project(0) + project(1) + project(2) + project(3)
             if s == 6 + Y_DONE:
                 acc[...] += project(-1) + project(4)
         for s in range(last + O_LAG + 1, last + Y_DONE + 1):
             if s <= last + Y_LAG:
-                for slot in arrived(s - Y_LAG):
-                    y_relay(slot)
-            for slot in arrived(s - Y_DONE):
-                y_done(slot)
+                y_relay(s - Y_LAG)
+            y_done(s - Y_DONE)
 
     x_relay(0)
     qkv = acc[...] + project(5) + project(6)
@@ -523,8 +523,8 @@
             dma((13,)),
             dma((2,)),
             dma((5, 2, NZ // 2)),
-            dma((2, NZ)),
-            dma((NZ,)),
+            dma((2, NZ // 2 + 1)),
+            dma((NZ // 2 + 1,)),
             dma((3,)),
             dma((4,)),
             dma((2, 2)),

time: 69.6 us -> 69.3 us (level)
  no operation moved by 1% of the time
where the time goes in v8:
time: 69.3 us; the launch traced here: 69.2 us
  Pallas kernels  68.5 us (99%)
    pallas_call x1, Pallas kernels, shards(): pl.pallas_call(layer_kernel, name='layer', out_shape=(jax.ShapeDtypeStruc...  66.6 us
    pallas_call x1, Pallas kernels, shards(): pl.pallas_call(sum_kernel, name='total', out_shape=(jax.ShapeDtypeStruct(...  1.96 us

profile of v8, /device:TPU:1, one launch (start us, length us, event | category | flops | bytes accessed | tf_op | source)
XLA Modules:
  0.0 69.2 jit_solution(12995719758210590522)
XLA Ops:
  0.6 66.6 %layer.1 = (bf16[8,64,384]{2,1,0:T(8,128)(2,1)}, bf16[8,64,384]{2,1,0:T(8,128)(2,1)}, f32[2,512]{1,0:T(2,128)}) custom-call(bf16[512,3072]{1,0:T(8,128)(2,1)} %tokens.1, bf16[48,128]{1,0:T(8,128)(2,1)} %wq.1, bf16[48,128]{1,0:T(8,128)(2,1)} %wk_in.1, bf16[48,128]{1,0:T(8,128)(2,1)} %wv.1, bf16[48,128]{1,0:T(8,128)(2,1)} %bitcast.1), custom_call_target="tpu_custom_call" | custom-call | tf_op jit(solution)/shard_map/layer/pallas_call | solution.py:490
  67.2 2.0 %total.1 = (bf16[64,3072]{1,0:T(8,128)(2,1)}, f32[2,512]{1,0:T(2,128)}) custom-call(bf16[8,64,384]{2,1,0:T(8,128)(2,1)} %get-tuple-element.5.ours, bf16[8,64,384]{2,1,0:T(8,128)(2,1)} %get-tuple-element.6.theirs, f32[2,512]{1,0:T(2,128)} %get-tuple-element.7.lse), custom_call_target="tpu_custom_call" | custom-call | tf_op jit(solution)/shard_map/total/pallas_call | solution.py:540
